TPU v7x, 32 devices: a whole 2x2x4 slice. The times are simulated.
32 devices in a mesh: sp: 16 (over z, y, x), tp: 2 (over core).
Axes of the slice: x: 2, y: 2, z: 4, core: 2. Of those that a mesh axis runs over, the one named last changes fastest.
Arguments:
- queries: bfloat16 [4096, 2048], P('sp', 'tp'), may hold values from -6 to 6
- keys: bfloat16 [4096, 2048], P('sp', 'tp'), may hold values from -6 to 6
- hidden: bfloat16 [4096, 2048], P('sp'), may hold values from -6 to 6
- value_weight: bfloat16 [2048, 2048], P(None, 'tp'), may hold values from -0.125 to 0.125
- beta_pre: float32 [4096, 16], P('sp', 'tp'), may hold values from -9 to 3
- decay_pre: float32 [4096, 16], P('sp', 'tp'), may hold values from -5 to 4
- decay_rate: float32 [16], P('tp'), may hold values from 0 to 0.06
- out_grad: bfloat16 [4096, 2048], P('sp', 'tp'), may hold values from -6 to 6
Outputs:
- d_queries: bfloat16 [4096, 2048], P('sp', 'tp')
- d_keys: bfloat16 [4096, 2048], P('sp', 'tp')
- d_beta: float32 [4096, 16], P('sp', 'tp')
- d_decay: float32 [4096, 16], P('sp', 'tp')
- d_hidden: bfloat16 [4096, 2048], P(('sp', 'tp'))
- d_weight: float32 [2048, 2048], P('sp', 'tp')
All inputs are finite; a program needn't handle non-finite values.
Results may differ from a plain program's by a relative error of at most 0.022.
Values may be sent and summed in bfloat16 or wider, within the bound.
A program may use at most 256 MiB of HBM per device.

v0:
```python
import jax
import jax.numpy as jnp
from jax import lax
from jax.sharding import PartitionSpec as P

BLOCK = 64


highest = lax.Precision.HIGHEST
norm_floor = 16.0


def prefix(value, axis, join, neutral, backward):
    count = lax.axis_size(axis)
    place = lax.axis_index(axis)
    ahead = count - 1 - place if backward else place
    gathered = jax.tree.map(
        lambda a, kind: lax.all_gather(a.astype(kind), axis),
        value,
        jax.tree.map(lambda a: jnp.bfloat16 if a.dtype == jnp.float32 else a.dtype, value),
    )
    state = jax.tree.map(lambda a, e: jnp.zeros_like(a) + jnp.asarray(e, a.dtype), value, neutral)

    def one(step, state):
        source = count - 1 - step if backward else step
        return join(
            state,
            jax.tree.map(
                lambda a, own: lax.dynamic_index_in_dim(a, source, 0, False).astype(own.dtype),
                gathered,
                value,
            ),
        )

    return lax.fori_loop(0, ahead, one, state)


def to_blocks(tensor, blocks):
    shaped = tensor.reshape((blocks, BLOCK) + tensor.shape[1:])
    return jnp.moveaxis(shaped, 1, 2)


def block_setup(key_raw, beta_pre, decay_pre, rate):
    blocks = key_raw.shape[0] // BLOCK
    key_unit = key_raw * lax.rsqrt(jnp.sum(key_raw * key_raw, axis=-1, keepdims=True) + norm_floor)
    write_rate = jax.nn.sigmoid(beta_pre)
    log_decay = -rate[None, :] * jax.nn.softplus(decay_pre)
    key_blocks = to_blocks(key_unit, blocks)
    rate_blocks = to_blocks(write_rate, blocks)
    log_sums = jnp.cumsum(to_blocks(log_decay, blocks), axis=-1)
    position = jnp.arange(BLOCK)
    inclusive = position[:, None] >= position[None, :]
    strict = position[:, None] > position[None, :]
    spread = log_sums[..., :, None] - log_sums[..., None, :]
    decay_mask = jnp.where(inclusive, jnp.exp(jnp.where(inclusive, spread, 0.0)), 0.0)
    key_gram = jnp.einsum("nhid,nhjd->nhij", key_blocks, key_blocks, precision=highest)
    lower_part = jnp.where(strict, rate_blocks[..., :, None] * key_gram * decay_mask, 0.0)
    system = jnp.eye(BLOCK, dtype=jnp.float32) + lower_part
    return (key_blocks, rate_blocks, log_sums, decay_mask, system)


def span_pieces(query_raw, key_raw, values, beta_pre, decay_pre, rate):
    key_blocks, rate_blocks, log_sums, decay_mask, system = block_setup(
        key_raw, beta_pre, decay_pre, rate
    )
    blocks = key_blocks.shape[0]
    query_unit = query_raw * lax.rsqrt(
        jnp.sum(query_raw * query_raw, axis=-1, keepdims=True) + norm_floor
    )
    query_unit = query_unit * query_raw.shape[-1] ** (-0.5)
    query_blocks = to_blocks(query_unit, blocks)
    value_blocks = to_blocks(values, blocks)
    block_gain = jnp.exp(log_sums)
    right_side = jnp.concatenate(
        [rate_blocks[..., None] * value_blocks, (rate_blocks * block_gain)[..., None] * key_blocks],
        axis=-1,
    )
    solved = jax.scipy.linalg.solve_triangular(system, right_side, lower=True, unit_diagonal=True)
    value_size = values.shape[-1]
    query_key = (
        jnp.einsum("nhid,nhjd->nhij", query_blocks, key_blocks, precision=highest) * decay_mask
    )
    query_decayed = query_blocks * block_gain[..., None]
    key_decayed = key_blocks * jnp.exp(log_sums[..., -1:] - log_sums)[..., None]
    pieces = (
        solved[..., :value_size],
        solved[..., value_size:],
        query_key,
        query_decayed,
        key_decayed,
        block_gain[..., -1],
    )
    return (pieces, (system, rate_blocks))


def sweep_pieces(pieces, carry_state):

    def sweep_advance(current, inputs):
        new_values, key_sweep, query_key, query_decayed, key_decayed, end_gain = inputs
        written = new_values - jnp.einsum("hcd,hde->hce", key_sweep, current, precision=highest)
        output = jnp.einsum("hcd,hde->hce", query_decayed, current, precision=highest)
        output = output + jnp.einsum("hij,hje->hie", query_key, written, precision=highest)
        current = end_gain[:, None, None] * current + jnp.einsum(
            "hcd,hce->hde", key_decayed, written, precision=highest
        )
        return (current, output)

    final, outputs = lax.scan(sweep_advance, carry_state, pieces)
    outputs = jnp.moveaxis(outputs, 2, 1)
    return (
        outputs.reshape(outputs.shape[0] * outputs.shape[1], outputs.shape[2], outputs.shape[3]),
        final,
    )


def span_transition(pieces):
    key_sweep, key_decayed, end_gain = (pieces[1], pieces[4], pieces[5])
    head_count, key_size = (key_sweep.shape[1], key_sweep.shape[3])

    def span_advance(transition, inputs):
        sweep, decayed, gain = inputs
        mixed = jnp.einsum("hce,hef->hcf", sweep, transition, precision=highest)
        updated = gain[:, None, None] * transition - jnp.einsum(
            "hcd,hcf->hdf", decayed, mixed, precision=highest
        )
        return (updated, None)

    identity = jnp.broadcast_to(
        jnp.eye(key_size, dtype=jnp.float32), (head_count, key_size, key_size)
    )
    final, _ = lax.scan(span_advance, identity, (key_sweep, key_decayed, end_gain))
    return final


def chain_forward(earlier, later):
    product = jnp.einsum("hde,hef->hdf", later[0], earlier[0], precision=highest)
    offset = jnp.einsum("hde,hef->hdf", later[0], earlier[1], precision=highest) + later[1]
    return (product, offset)


def chain_backward(earlier, later):
    product = jnp.einsum("hde,hef->hdf", later[0], earlier[0], precision=highest)
    offset = later[1] + jnp.einsum("hde,hef->hdf", later[0], earlier[1], precision=highest)
    return (product, offset)


def weight_term(hidden, grad_list):
    total = lax.dot_general(
        hidden, grad_list[0], (((0,), (0,)), ((), ())), preferred_element_type=jnp.float32
    )
    for extra in grad_list[1:]:
        total = total + lax.dot_general(
            hidden, extra, (((0,), (0,)), ((), ())), preferred_element_type=jnp.float32
        )
    return total


def per_device(queries, keys, hidden, value_weight, beta_pre, decay_pre, decay_rate, out_grad):
    head_count = decay_rate.shape[0]
    key_size = queries.shape[1] // head_count
    value_size = value_weight.shape[1] // head_count
    length = queries.shape[0]
    blocks = length // BLOCK
    values = jnp.dot(hidden, value_weight, preferred_element_type=jnp.float32).astype(jnp.bfloat16)
    query_raw = queries.astype(jnp.float32).reshape(length, head_count, key_size)
    key_raw = keys.astype(jnp.float32).reshape(length, head_count, key_size)
    value_heads = values.astype(jnp.float32).reshape(length, head_count, value_size)
    grad_heads = out_grad.astype(jnp.float32).reshape(length, head_count, value_size)
    zero_state = jnp.zeros((head_count, key_size, value_size), jnp.float32)

    def make_pieces(query_in, key_in, value_in, beta_in, decay_in):
        return span_pieces(query_in, key_in, value_in, beta_in, decay_in, decay_rate)

    primal = (query_raw, key_raw, value_heads, beta_pre, decay_pre)
    pieces, pull_pieces, extras = jax.vjp(make_pieces, *primal, has_aux=True)
    system, rate_blocks = extras

    def value_solve(value_in):
        scaled = rate_blocks[..., None] * to_blocks(value_in, blocks)
        return jax.scipy.linalg.solve_triangular(system, scaled, lower=True, unit_diagonal=True)

    _, pull_values = jax.vjp(value_solve, value_heads)
    (_, span_offset), pull_zero = jax.vjp(sweep_pieces, pieces, zero_state)
    local_cot, own_state_grad = pull_zero((grad_heads, zero_state))
    value_local = pull_values(local_cot[0])[0]
    local_grad = value_local.reshape(length, head_count * value_size).astype(jnp.bfloat16)
    transition = span_transition(pieces)
    identity = jnp.broadcast_to(jnp.eye(key_size, dtype=jnp.float32), transition.shape)
    earlier_maps = prefix(
        (transition, span_offset), "sp", chain_forward, (identity, zero_state), False
    )
    start_state = earlier_maps[1]
    later_maps = prefix(
        (jnp.swapaxes(transition, 1, 2), own_state_grad),
        "sp",
        chain_backward,
        (identity, zero_state),
        True,
    )
    end_grad = later_maps[1]
    _, pull_full = jax.vjp(sweep_pieces, pieces, start_state)
    total_cot = pull_full((grad_heads, end_grad))[0]
    carried_cot = jax.tree.map(lambda first, second: first - second, total_cot, local_cot)
    grad_query, grad_key, _, grad_beta, grad_decay = pull_pieces(total_cot)
    value_carried = pull_values(carried_cot[0])[0]
    carried_grad = value_carried.reshape(length, head_count * value_size).astype(jnp.bfloat16)
    d_weight = lax.psum_scatter(
        weight_term(hidden, [local_grad, carried_grad]), "sp", scatter_dimension=0, tiled=True
    )
    total = lax.dot_general(
        local_grad, value_weight, (((1,), (1,)), ((), ())), preferred_element_type=jnp.float32
    )
    d_hidden = lax.psum_scatter(
        (
            total
            + lax.dot_general(
                carried_grad,
                value_weight,
                (((1,), (1,)), ((), ())),
                preferred_element_type=jnp.float32,
            )
        ).astype(jnp.bfloat16),
        "tp",
        scatter_dimension=0,
        tiled=True,
    )
    d_queries = grad_query.reshape(length, head_count * key_size).astype(jnp.bfloat16)
    d_keys = grad_key.reshape(length, head_count * key_size).astype(jnp.bfloat16)
    return (d_queries, d_keys, grad_beta, grad_decay, d_hidden, d_weight)


def solution(mesh):
    return jax.shard_map(
        per_device,
        mesh=mesh,
        in_specs=(
            P("sp", "tp"),
            P("sp", "tp"),
            P("sp", None),
            P(None, "tp"),
            P("sp", "tp"),
            P("sp", "tp"),
            P("tp"),
            P("sp", "tp"),
        ),
        out_specs=(
            P("sp", "tp"),
            P("sp", "tp"),
            P("sp", "tp"),
            P("sp", "tp"),
            P(("sp", "tp"), None),
            P("sp", "tp"),
        ),
        check_vma=False,
    )
```

profile of v0, /device:TPU:0, one launch (start us, length us, event | category | flops | bytes accessed | tf_op | source)
XLA Modules:
  0.0 823.7 jit_solution(2084794772031629973)
XLA Ops:
  12.5 2.3 fusion.130
  14.8 2.3 fusion.118
  19.0 158.0 %custom-call.13 = f32[4,8,1,64,64]{3,4,2,1,0:T(8,128)S(1)} custom-call(f32[4,8,1,64,64]{4,3,2,1,0:T(8,128)} %get-tuple-element.1072), custom_call_target="InvertDiagBlocksLowerTriangular" | custom-call | tf_op jit(solution)/shard_map/jvp(jit(_solve_triangular))/vmap(vmap())/triangular_solve | solution.py:78
  177.1 3.7 fusion.111
  187.9 17.2 %while.108 = (s32[]{:T(128)}, f32[8,128,128]{2,1,0:T(8,128)S(1)}, f32[4,8]{1,0:T(4,128)}, f32[4,8,64,128]{3,2,1,0:T(8,128)}, f32[4,8,64,128]{3,2,1,0:T(8,128)}, /*index=5*/s32[]{:T(128)}) while((s32[]{:T(128)}, f32[8,128,128]{2,1,0:T(8,128)S(1)}, f32[4,8]{1,0:T(4,128)}, f32[4,8,64,128]{3,2,1,0:T(8,128)}, f32[4,8,64,128]{3,2,1,0:T(8,128)}, ...), condition=%wide.region_3.4_spmd, body=%wide.region_2.3_spmd.sunk | while | flops 201588736 | bytes 2622633 | solution.py:131
  190.1 2.1 convolution_subtract_fusion.5
  194.4 2.1 convolution_subtract_fusion.5
  198.7 2.1 convolution_subtract_fusion.5
  203.0 2.1 convolution_subtract_fusion.5
  207.2 22.1 %while.113 = (s32[]{:T(128)}, f32[8,128,128]{2,1,0:T(8,128)S(1)}, f32[4,8,1,1]{1,3,2,0:T(1,128)}, f32[4,8]{1,0:T(4,128)}, f32[4,8,64,128]{3,2,1,0:T(8,128)}, /*i...) while((s32[]{:T(128)}, f32[8,128,128]{2,1,0:T(8,128)S(1)}, ...), condition=%wide.region_6.7_spmd.clone, body=%wide.region_5.6_spmd.clone.sunk | while | flops 201916416 | bytes 2886860 | solution.py:108
  226.1 2.1 convolution_add_fusion.28
  230.2 2.5 copy.116
  237.0 36.7 %while.114 = (s32[]{:T(128)}, f32[8,128,128]{2,1,0:T(8,128)}, f32[4,8,64,128]{3,2,1,0:T(8,128)}, f32[4,8,1,1]{1,3,2,0:T(1,128)}, f32[4,8,64,128]{3,2,1,0:T(8,128...) while((s32[]{:T(128)}, f32[8,128,128]{2,1,0:T(8,128)}, ...), condition=%wide.region_8.9_spmd.clone, body=%wide.region_7.8_spmd.clone.sunk | while | flops 353107968 | bytes 7606003 | solution.py:108
  238.6 2.1 bitcast_dynamic-update-slice_fusion.11
  243.3 2.8 convolution_add_fusion.30
  247.8 2.1 bitcast_dynamic-update-slice_fusion.11
  252.5 2.8 convolution_add_fusion.30
  261.7 2.8 convolution_add_fusion.30
  266.2 2.1 bitcast_dynamic-update-slice_fusion.11
  270.9 2.8 convolution_add_fusion.30
  273.7 2.1 convert_element_type.87
  276.5 2.7 fusion.113
  280.4 5.6 fusion.146
  286.0 75.6 %all-gather.15.cloned.1.call-done = bf16[128,128,128]{2,1,0:T(8,128)(2,1)} async-done(((bf16[8,128,128]{2,1,0:T(8,128)(2,1)}), bf16[128,128,128]{2,1,0:T(8,128)(2,1)}) %all-gather.15.cloned.1.call-update) | async-done | bytes 4194320 | tf_op jit(solution)/shard_map/all_gather | solution.py:18
  362.8 26.2 %while.111 = (s32[]{:T(128)}, f32[8,128,128]{2,1,0:T(8,128)S(1)}, f32[4,8,128,128]{3,2,1,0:T(8,128)}, f32[4,8,64,128]{3,2,1,0:T(8,128)}, f32[4,8,1,1]{1,3,2,0:T(...) while((s32[]{:T(128)}, f32[8,128,128]{2,1,0:T(8,128)S(1)}, ...), condition=%wide.region_14.15_spmd, body=%wide.region_13.14_spmd.sunk | while | flops 201654272 | bytes 4197101 | solution.py:108
  362.8 2.3 bitcast_dynamic-update-slice_fusion.8
  366.6 2.1 convolution_add_fusion.25
  369.3 2.3 bitcast_dynamic-update-slice_fusion.8
  373.1 2.1 convolution_add_fusion.25
  375.9 2.3 bitcast_dynamic-update-slice_fusion.8
  382.4 2.3 bitcast_dynamic-update-slice_fusion.8
  386.3 2.1 convolution_add_fusion.25
  389.0 50.2 %all-gather.9.cloned.1.call-done = bf16[128,128,128]{2,1,0:T(8,128)(2,1)} async-done(((bf16[8,128,128]{2,1,0:T(8,128)(2,1)}), bf16[128,128,128]{2,1,0:T(8,128)(2,1)}) %all-gather.9.cloned.1.call-update) | async-done | bytes 4194320 | tf_op jit(solution)/shard_map/all_gather | solution.py:18
  439.2 77.4 %all-gather.11.cloned.1.call-done = bf16[128,128,128]{2,1,0:T(8,128)(2,1)} async-done(((bf16[8,128,128]{2,1,0:T(8,128)(2,1)}), bf16[128,128,128]{2,1,0:T(8,128)(2,1)}) %all-gather.11.cloned.1.call-update) | async-done | bytes 4194320 | tf_op jit(solution)/shard_map/all_gather | solution.py:18
  516.6 23.0 %while.109 = (s32[]{:T(128)}, f32[8,128,128]{2,1,0:T(8,128)S(1)}, s32[]{:T(128)}, bf16[16,8,128,128]{3,2,1,0:T(8,128)(2,1)}, bf16[16,8,128,128]{3,2,1,0:T(8,128)...) while((s32[]{:T(128)}, f32[8,128,128]{2,1,0:T(8,128)S(1)}, s32[]{:T(128)}, ...), condition=%wide.region_10.11_spmd, body=%wide.region_9.10_spmd.sunk | while | flops 201588736 | bytes 2622603 | solution.py:35
  545.2 71.6 %while.112 = (s32[]{:T(128)}, f32[8,128,128]{2,1,0:T(8,128)S(1)}, f32[4,8,64,128]{3,2,1,0:T(8,128)}, f32[4,8,64,128]{3,2,1,0:T(8,128)}, f32[4,8,64,64]{3,2,1,0:T...) while((s32[]{:T(128)}, f32[8,128,128]{2,1,0:T(8,128)S(1)}, ...), condition=%wide.region_17.18_spmd, body=%wide.region_15.17_spmd.sunk | while | flops 705495040 | bytes 18882472 | solution.py:108
  546.9 2.1 bitcast_dynamic-update-slice_fusion.10
  551.2 2.8 fusion.287
  557.8 2.9 fusion.286
  560.8 2.3 fusion.285
  564.8 2.1 bitcast_dynamic-update-slice_fusion.10
  569.1 2.8 fusion.287
  575.7 2.9 fusion.286
  578.7 2.3 fusion.285
  582.6 2.1 bitcast_dynamic-update-slice_fusion.10
  587.0 2.8 fusion.287
  593.6 3.0 fusion.286
  596.6 2.3 fusion.285
  600.6 2.1 bitcast_dynamic-update-slice_fusion.10
  604.9 2.8 fusion.287
  611.6 3.0 fusion.286
  614.5 2.3 fusion.285
  616.8 3.1 fusion.112
  621.0 8.0 add_bitcast_fusion
  629.8 5.5 fusion.148
  639.4 4.2 fusion.101
  643.6 3.4 multiply_select_fusion
  648.8 2.6 reduce_window_sum.23
  652.9 4.8 fusion.104
  657.7 2.8 convolution_add_fusion.12
  664.2 5.4 fusion.96
  669.7 4.2 broadcast_multiply_fusion
  683.3 119.6 %reduce-scatter.5.cloned.1.call-done = f32[128,1024]{0,1:T(8,128)} async-done(((f32[2048,1024]{0,1:T(8,128)}), f32[128,1024]{0,1:T(8,128)}) %reduce-scatter.5.cloned.1.call-update) | async-done | bytes 524304 | tf_op jit(solution)/shard_map/reduce_scatter | solution.py:207
  804.9 11.5 %reduce-scatter.3.cloned.1.call-done = bf16[128,2048]{1,0:T(8,128)(2,1)} async-done(((bf16[256,2048]{1,0:T(8,128)(2,1)}), bf16[128,2048]{1,0:T(8,128)(2,1)}) %reduce-scatter.3.cloned.1.call-update) | async-done | bytes 524304 | tf_op jit(solution)/shard_map/reduce_scatter | solution.py:213
  (332 shorter events, 165.9 us)
Async XLA Ops:
  7.2 169.9 %copy-start = (bf16[256,2048]{1,0:T(8,128)(2,1)S(1)}, bf16[256,2048]{1,0:T(8,128)(2,1)}, u32[]{:S(2)}) copy-start(bf16[256,2048]{1,0:T(8,128)(2,1)} %param.26) | copy-start | bytes 3145732
  7.2 278.8 %all-gather.13.cloned.1.call-start = ((), (), s32[]{:S(2)}) async-start(), calls=%async_computation.6 | async-start | bytes 4456448 | tf_op jit(solution)/shard_map/all_gather | solution.py:18
  7.2 10.0 %copy-start.36 = (pred[64,64]{1,0:T(8,128)(4,1)}, pred[64,64]{1,0:T(8,128)(4,1)S(1)}, u32[]{:S(2)}) copy-start(pred[64,64]{1,0:T(8,128)(4,1)S(1)} %get-tuple-element.1082) | copy-start | bytes 12292
  8.5 1.0 copy-start.29
  9.2 1.1 copy-start.32
  9.7 1.4 copy-start.50
  9.7 1.4 copy-start.46
  9.7 1.5 copy-start.44
  9.9 7.3 copy-start.3
  10.4 0.6 copy-start.34
  11.1 6.1 copy-start.48
  11.4 5.8 copy-start.38
  14.8 4.2 copy-start.22
  17.2 1.8 copy-start.15
  177.0 6.2 copy-start.7
  181.1 2.1 copy-start.17
  185.2 2.0 copy-start.10
  205.3 2.0 copy-start.27
  206.1 155.5 %all-gather.15.cloned.1.call-start = ((), (), s32[]{:S(2)}) async-start(), calls=%async_computation.7 | async-start | bytes 4456448 | tf_op jit(solution)/shard_map/all_gather | solution.py:18
  229.3 3.4 copy-start.31
  230.1 209.1 %all-gather.9.cloned.1.call-start = ((), (), s32[]{:S(2)}) async-start(), calls=%async_computation.4 | async-start | bytes 4456448 | tf_op jit(solution)/shard_map/all_gather | solution.py:18
  233.0 1.2 copy-start.4
  237.0 4.3 copy-start.2
  246.1 4.5 copy-start.2
  255.3 4.5 copy-start.2
  264.5 4.5 copy-start.2
  273.7 6.7 copy-start.1
  275.9 240.7 %all-gather.11.cloned.1.call-start = ((), (), s32[]{:S(2)}) async-start(), calls=%async_computation.5 | async-start | bytes 4456448 | tf_op jit(solution)/shard_map/all_gather | solution.py:18
  276.4 526.4 %reduce-scatter.5.cloned.1.call-start = ((), (), s32[]{:S(2)}) async-start(), calls=%async_computation.3 | async-start | bytes 8912896 | tf_op jit(solution)/shard_map/reduce_scatter | solution.py:207
  545.2 5.9 copy-start.6
  563.1 5.9 copy-start.6
  580.9 5.9 copy-start.6
  598.9 5.9 copy-start.6
  620.2 0.8 copy-start.26
  629.0 0.7 copy-start.33
  629.0 187.4 %reduce-scatter.3.cloned.1.call-start = ((), (), s32[]{:S(2)}) async-start(), calls=%async_computation.2 | async-start | bytes 1572864 | tf_op jit(solution)/shard_map/reduce_scatter | solution.py:213
  629.8 5.6 copy-start.8
  629.8 5.6 copy-start.11
  629.8 5.6 copy-start.14
  635.4 2.0 copy-start.18
  635.4 2.0 copy-start.24
  637.3 1.7 copy-start.13
  639.3 4.2 copy-start.9
  639.3 4.2 copy-start.12
  639.3 4.2 copy-start.16
  639.3 4.3 copy-start.23
  639.3 4.3 copy-start.37
  639.4 4.3 copy-start.39
  643.6 3.8 copy-start.5
  643.6 3.8 copy-start.21
  647.0 1.1 copy-start.40
  647.0 1.1 copy-start.41
  652.9 4.8 copy-start.25
  662.8 1.0 copy-start.19
  674.0 1.1 copy-start.35
  674.6 3.4 copy-start.42
  675.0 2.4 copy-start.43
  675.0 2.4 copy-start.45
  675.0 3.0 copy-start.47
  675.0 3.0 copy-start.49
  675.4 4.0 copy-start.20
  675.4 4.0 copy-start.28
  680.8 1.1 copy-start.30
Sparse Core Ops, SparseCore 0:
  206.3 78.3 all-gather.12
  287.4 74.1 all-gather.14
  364.9 74.1 all-gather.8
  442.4 74.1 all-gather.10
  629.1 173.7 reduce-scatter.4
  805.5 10.8 reduce-scatter.2
where the time goes:
time: 835 us; the launch traced here: 824 us
  waiting for transfers between devices  335 us (40%)
  matrix products  236 us (28%)
  other arithmetic  181 us (22%)
  local copies, waits for them, and re-layouts  53.3 us (6%)
  between operations  15.5 us (2%)
    all_gather x4, waiting for transfers between devices, prefix(): lax.all_gather(a.astype(kind), axis)  203 us
    another operation x4, other arithmetic, span_pieces(): jax.scipy.linalg.solve_triangular(system, right_side, lower=True, unit_di...  158 us
    reduce_scatter x1, waiting for transfers between devices, per_device(): lax.psum_scatter(weight_term(hidden, [local_grad, carried_grad]), 'sp', s...  120 us
    dot_general x20, matrix products, sweep_advance(): jnp.einsum('hcd,hde->hce', key_sweep, current, precision=highest)  41.9 us
    dot_general x20, matrix products, sweep_advance(): jnp.einsum('hcd,hce->hde', key_decayed, written, precision=highest)  41.1 us
    dot_general x12, matrix products, sweep_advance(): jnp.einsum('hcd,hde->hce', query_decayed, current, precision=highest)  27.8 us
    dot_general x12, matrix products, sweep_advance(): jnp.einsum('hij,hje->hie', query_key, written, precision=highest)  25.8 us
    dot_general x15, matrix products, chain_backward(): jnp.einsum('hde,hef->hdf', later[0], earlier[1], precision=highest)  21.7 us
  transfers between devices with their start and end apart: 6, of which 5 were waited for; matrix products, arithmetic and copies ran while one was open for 19% of the time, Pallas kernels for 0%

commit v1 on v0

v1 whole, which is shorter than its diff:
```python
import functools

import jax
import jax.numpy as jnp
from jax import lax
from jax.experimental import pallas as pl
from jax.experimental.pallas import tpu as pltpu
from jax.sharding import PartitionSpec as P

f32 = jnp.float32
bf16 = jnp.bfloat16
norm_floor = 16.0


def mm(a, b, ca, cb):
    return lax.dot_general(
        a.astype(bf16), b.astype(bf16), (((ca,), (cb,)), ((), ())), preferred_element_type=f32
    )


def nn(a, b):
    return mm(a, b, 1, 0)


def nt(a, b):
    return mm(a, b, 1, 1)


def tn(a, b):
    return mm(a, b, 0, 0)


def nn3(a, b):
    a_hi, b_hi = a.astype(bf16), b.astype(bf16)
    a_lo, b_lo = a - a_hi.astype(f32), b - b_hi.astype(f32)
    return nn(a_hi, b_hi) + (nn(a_hi, b_lo) + nn(a_lo, b_hi))


def invert_unit_lower(low):
    size = low.shape[0]
    base = min(size, 128)
    ii = lax.broadcasted_iota(jnp.int32, (base, base), 0)
    jj = lax.broadcasted_iota(jnp.int32, (base, base), 1)
    masks = []
    width = 1
    while width < base:
        masks.append((ii // (2 * width) == jj // (2 * width)) & (ii // width != jj // width))
        width *= 2
    parts = []
    for start in range(0, size, base):
        block = low[start : start + base, start : start + base]
        inverse = jnp.where(ii == jj, 1.0, 0.0) - jnp.where(masks[0], block, 0.0)
        parts.append([block, inverse])
    for mask in masks[1:]:
        for part in parts:
            off = jnp.where(mask, part[0], 0.0)
            part[1] = part[1] - nn3(part[1], nn3(off, part[1]))
    inverses = [part[1] for part in parts]
    while len(inverses) > 1:
        joined = []
        width = inverses[0].shape[0]
        for pair in range(0, len(inverses), 2):
            first, second = inverses[pair], inverses[pair + 1]
            row = (pair + 1) * width
            cross = low[row : row + width, row - width : row]
            corner = -nn3(second, nn3(cross, first))
            top = jnp.concatenate([first, jnp.zeros_like(first)], axis=1)
            joined.append(
                jnp.concatenate([top, jnp.concatenate([corner, second], axis=1)], axis=0)
            )
        inverses = joined
    return inverses[0]


def unit(raw):
    return lax.rsqrt(jnp.sum(raw * raw, axis=-1, keepdims=True) + norm_floor)


def order(size):
    ii = lax.broadcasted_iota(jnp.int32, (size, size), 0)
    jj = lax.broadcasted_iota(jnp.int32, (size, size), 1)
    return ii >= jj, ii > jj


def first_phase(qr, kr, v, do, b, gc, gr, ge):
    width = qr.shape[1]
    q = qr * (unit(qr) * width ** (-0.5))
    k = kr * unit(kr)
    inclusive, strict = order(qr.shape[0])
    mask = jnp.where(inclusive, jnp.exp(jnp.minimum(gc - gr, 0.0)), 0.0)
    low = jnp.where(strict, b * nt(k, k) * mask, 0.0)
    inverse = invert_unit_lower(low)
    eg = jnp.exp(gc)
    kd = k * jnp.exp(ge - gc)
    uw = nn(inverse, jnp.concatenate([b * v, (b * eg) * k], axis=1))
    qk = nt(q, k) * mask
    moved = tn(kd, uw)
    ii = lax.broadcasted_iota(jnp.int32, (width, width), 0)
    jj = lax.broadcasted_iota(jnp.int32, (width, width), 1)
    dv = v.shape[1]
    offset = moved[:, :dv]
    transition = jnp.where(ii == jj, jnp.exp(ge), 0.0) - moved[:, dv:]
    dw0 = tn(qk, do)
    own = tn(q * eg, do) - tn(uw[:, dv:], dw0)
    return inverse, uw, dw0, transition, offset, own


def value_phase(kr, inverse, dw0, end, b, gc, ge):
    kd = kr * (unit(kr) * jnp.exp(ge - gc))
    return tn(inverse, dw0 + nn(kd, end))


def last_phase(qr, kr, v, do, uw, dr, start, end, b, gc, gr, ge):
    width = qr.shape[1]
    dv = v.shape[1]
    rq, rk = unit(qr), unit(kr)
    scale = width ** (-0.5)
    q = qr * (rq * scale)
    k = kr * rk
    inclusive, strict = order(qr.shape[0])
    mask = jnp.where(inclusive, jnp.exp(jnp.minimum(gc - gr, 0.0)), 0.0)
    gram = jnp.where(strict, nt(k, k) * mask, 0.0)
    qk = nt(q, k) * mask
    eg = jnp.exp(gc)
    ekd = jnp.exp(ge - gc)
    rest = v - eg * nn(k, start)
    written = uw[:, :dv] - nn(uw[:, dv:], start)
    dp = nt(do, written)
    dqd = nt(do, start) * eg
    dkd = nt(written, end) * ekd
    dl = -nt(dr, written)
    dkg = nt(dr, start) * (-b * eg)
    dlg = dl * gram
    db = jnp.sum(dr * rest, axis=1, keepdims=True) + jnp.sum(dlg, axis=1, keepdims=True)
    dg = jnp.where(strict, dl * b * mask, 0.0)
    dqk = dp * mask
    logs = dlg * b + dp * qk
    dq = nn(dqk, k) + dqd
    dk = tn(dqk, q) + nn(dg, k) + tn(dg, k) + dkg + dkd
    kept = jnp.sum(dkd * k, axis=1, keepdims=True)
    gcol = jnp.sum(logs, axis=1, keepdims=True) + jnp.sum(dqd * q + dkg * k, axis=1, keepdims=True) - kept
    last = jnp.sum(kept, axis=0, keepdims=True) + jnp.exp(ge) * jnp.sum(
        jnp.sum(start * end, axis=1, keepdims=True), axis=0, keepdims=True
    )
    rows = lax.broadcasted_iota(jnp.int32, gcol.shape, 0)
    gcol = gcol + jnp.where(rows == gcol.shape[0] - 1, last, 0.0)
    grow = jnp.sum(logs, axis=0, keepdims=True)
    dqr = (rq * scale) * (dq - qr * (rq * rq * jnp.sum(qr * dq, axis=1, keepdims=True)))
    dkr = rk * (dk - kr * (rk * rk * jnp.sum(kr * dk, axis=1, keepdims=True)))
    return dqr, dkr, db, gcol, grow


def pick(ref, head):
    table = ref[...]
    lane = lax.broadcasted_iota(jnp.int32, table.shape, 1)
    return jnp.sum(jnp.where(lane == head, table, 0.0), axis=1, keepdims=True)


def put(ref, head, column):
    lane = lax.broadcasted_iota(jnp.int32, ref.shape, 1)
    ref[...] = jnp.where(lane == head, column, ref[...])


def gains(g_ref, row_ref, head):
    gr = row_ref[0]
    return pick(g_ref, head), gr, gr[:, gr.shape[1] - 1 :]


def first_kernel(q, k, v, do, b, g, row, inv_o, uw_o, dw_o, t_o, off_o, own_o):
    head = pl.program_id(0)
    gc, gr, ge = gains(g, row, head)
    inverse, uw, dw0, transition, offset, own = first_phase(
        q[...].astype(f32), k[...].astype(f32), v[...].astype(f32), do[...].astype(f32),
        pick(b, head), gc, gr, ge,
    )
    inv_o[0] = inverse.astype(inv_o.dtype)
    uw_o[0] = uw
    dw_o[0] = dw0
    t_o[0] = transition.astype(bf16)
    off_o[0] = offset.astype(bf16)
    own_o[0] = own.astype(bf16)


def value_kernel(k, inv, dw, end, b, g, row, dr_o, dv_o):
    head = pl.program_id(0)
    gc, gr, ge = gains(g, row, head)
    bc = pick(b, head)
    dr = value_phase(k[...].astype(f32), inv[0], dw[0], end[0], bc, gc, ge)
    dr_o[0] = dr
    dv_o[...] = (bc * dr).astype(bf16)


def last_kernel(q, k, v, do, uw, dr, start, end, b, g, row, dq_o, dk_o, db_o, gc_o, gr_o):
    head = pl.program_id(0)
    gc, gr, ge = gains(g, row, head)
    dqr, dkr, db, gcol, grow = last_phase(
        q[...].astype(f32), k[...].astype(f32), v[...].astype(f32), do[...].astype(f32),
        uw[0], dr[0], start[0].astype(f32), end[0].astype(f32), pick(b, head), gc, gr, ge,
    )
    dq_o[...] = dqr.astype(bf16)
    dk_o[...] = dkr.astype(bf16)

    @pl.when(head == 0)
    def _():
        db_o[...] = jnp.zeros_like(db_o)
        gc_o[...] = jnp.zeros_like(gc_o)

    put(db_o, head, db)
    put(gc_o, head, gcol)
    gr_o[0] = grow


def scan_kernel(count, t, off, own, start_o, end_o):
    shape = off.shape[1:]

    def split(a, b, ca):
        hi = b.astype(bf16)
        return mm(a, hi, ca, 0) + mm(a, b - hi.astype(f32), ca, 0)

    def step(i, carry):
        state, grad = carry
        j = count - 1 - i
        start_o[i] = state.astype(bf16)
        end_o[j] = grad.astype(bf16)
        state = split(t[i], state, 1) + off[i].astype(f32)
        grad = split(t[j], grad, 0) + own[j].astype(f32)
        return state, grad

    zero = jnp.zeros(shape, f32)
    lax.fori_loop(0, count, step, (zero, zero))


def per_device(queries, keys, hidden, value_weight, beta_pre, decay_pre, decay_rate, out_grad):
    heads = decay_rate.shape[0]
    length, dk = queries.shape[0], queries.shape[1] // heads
    dv = value_weight.shape[1] // heads
    count = lax.axis_size("sp")
    parts = count // heads
    cols = dv // parts

    values = jnp.dot(hidden, value_weight, preferred_element_type=f32).astype(bf16)
    beta = jax.nn.sigmoid(beta_pre)
    log_decay = -decay_rate[None, :] * jax.nn.softplus(decay_pre)
    inclusive = jnp.tril(jnp.ones((length, length), f32))
    sums = jnp.dot(inclusive, log_decay, precision=lax.Precision.HIGHEST)
    sums_row = sums.T.reshape(heads, 1, length)

    wide = lambda n: pl.BlockSpec((length, n), lambda h: (0, h))
    per_head = lambda r, c: pl.BlockSpec((1, r, c), lambda h: (h, 0, 0))
    table = pl.BlockSpec((length, heads), lambda h: (0, 0))
    shape = jax.ShapeDtypeStruct
    params = pltpu.CompilerParams(dimension_semantics=("arbitrary",))

    inverse, uw, dw0, transition, offset, own = pl.pallas_call(
        first_kernel,
        grid=(heads,),
        in_specs=[wide(dk), wide(dk), wide(dv), wide(dv), table, table, per_head(1, length)],
        out_specs=[
            per_head(length, length), per_head(length, dv + dk), per_head(length, dv),
            per_head(dk, dk), per_head(dk, dv), per_head(dk, dv),
        ],
        out_shape=[
            shape((heads, length, length), bf16), shape((heads, length, dv + dk), f32),
            shape((heads, length, dv), f32), shape((heads, dk, dk), bf16),
            shape((heads, dk, dv), bf16), shape((heads, dk, dv), bf16),
        ],
        compiler_params=params,
        name="first",
    )(queries, keys, values, out_grad, beta, sums, sums_row)

    def by_owner(a):
        a = a.reshape(heads, dk, parts, cols)
        return jnp.moveaxis(a, 2, 1).reshape(count, dk, cols)

    packed = jnp.concatenate(
        [jnp.repeat(transition, parts, axis=0), by_owner(offset), by_owner(own)], axis=2
    )
    got = lax.all_to_all(packed, "sp", 0, 0, tiled=True)
    starts, ends = pl.pallas_call(
        functools.partial(scan_kernel, count),
        out_shape=[shape((count, dk, cols), bf16), shape((count, dk, cols), bf16)],
        name="scan",
    )(got[:, :, :dk], got[:, :, dk : dk + cols], got[:, :, dk + cols :])
    back = lax.all_to_all(jnp.concatenate([starts, ends], axis=2), "sp", 0, 0, tiled=True)
    back = jnp.moveaxis(back.reshape(heads, parts, dk, 2, cols), 1, 3).reshape(heads, dk, 2, dv)
    start, end = back[:, :, 0], back[:, :, 1]

    dr, grad_values = pl.pallas_call(
        value_kernel,
        grid=(heads,),
        in_specs=[
            wide(dk), per_head(length, length), per_head(length, dv), per_head(dk, dv),
            table, table, per_head(1, length),
        ],
        out_specs=[per_head(length, dv), wide(dv)],
        out_shape=[shape((heads, length, dv), f32), shape((length, heads * dv), bf16)],
        compiler_params=params,
        name="value",
    )(keys, inverse, dw0, end, beta, sums, sums_row)

    partial_weight = lax.dot_general(
        hidden, grad_values, (((0,), (0,)), ((), ())), preferred_element_type=f32
    )
    d_weight = lax.psum_scatter(
        partial_weight.astype(bf16), "sp", scatter_dimension=0, tiled=True
    ).astype(f32)
    partial_hidden = lax.dot_general(
        grad_values, value_weight, (((1,), (1,)), ((), ())), preferred_element_type=f32
    )
    d_hidden = lax.psum_scatter(
        partial_hidden.astype(bf16), "tp", scatter_dimension=0, tiled=True
    )

    d_queries, d_keys, db, gcol, grow = pl.pallas_call(
        last_kernel,
        grid=(heads,),
        in_specs=[
            wide(dk), wide(dk), wide(dv), wide(dv), per_head(length, dv + dk),
            per_head(length, dv), per_head(dk, dv), per_head(dk, dv),
            table, table, per_head(1, length),
        ],
        out_specs=[wide(dk), wide(dk), table, table, per_head(1, length)],
        out_shape=[
            shape(queries.shape, bf16), shape(keys.shape, bf16), shape((length, heads), f32),
            shape((length, heads), f32), shape((heads, 1, length), f32),
        ],
        compiler_params=params,
        cost_estimate=pl.CostEstimate(
            flops=heads * 13 * 2 * length * length * dk, bytes_accessed=12 << 20, transcendentals=0
        ),
        name="last",
    )(queries, keys, values, out_grad, uw, dr, start, end, beta, sums, sums_row)
    grad_sums = gcol - grow.reshape(heads, length).T
    grad_log = jnp.dot(inclusive.T, grad_sums, precision=lax.Precision.HIGHEST)
    d_decay = grad_log * (-decay_rate[None, :] * jax.nn.sigmoid(decay_pre))
    d_beta = db * beta * (1.0 - beta)
    return (d_queries, d_keys, d_beta, d_decay, d_hidden, d_weight)


def solution(mesh):
    return jax.shard_map(
        per_device,
        mesh=mesh,
        in_specs=(
            P("sp", "tp"), P("sp", "tp"), P("sp", None), P(None, "tp"),
            P("sp", "tp"), P("sp", "tp"), P("tp"), P("sp", "tp"),
        ),
        out_specs=(
            P("sp", "tp"), P("sp", "tp"), P("sp", "tp"), P("sp", "tp"),
            P(("sp", "tp"), None), P("sp", "tp"),
        ),
        check_vma=False,
    )
```

time: 835 us -> 240 us (0.29); the launches traced: 824 us -> 239 us
  waiting for transfers between devices: 335 us -> 80.1 us
  matrix products: 236 us -> 15.5 us
  other arithmetic: 181 us -> 4.42 us
  Pallas kernels: 0 us -> 52.8 us
  blocking collectives: 0 us -> 52.6 us
  local copies, waits for them, and re-layouts: 53.3 us -> 19.1 us
    dot_general x99 -> x5, matrix products: 223 us -> 15.5 us  [the longest x1 4.44 us: per_device(): lax.dot_general(grad_values, value_weight, (((1,), (1,)), ((), ())), pref...]
    all_gather x4 -> x0, waiting for transfers between devices: 203 us -> none  [prefix(): lax.all_gather(a.astype(kind), axis)]
    another operation x6 -> x1, other arithmetic: 162 us -> 0.11 us  [the longest x4 158 us: span_pieces(): jax.scipy.linalg.solve_triangular(system, right_side, lower=True, unit_di...]
    reduce_scatter x2 -> x1, waiting for transfers between devices: 131 us -> 8.67 us  [per_device(): lax.psum_scatter(partial_hidden.astype(bf16), 'tp', scatter_dimension=0,...]
    unnamed x6 -> x3, waiting for transfers between devices: 0.6 us -> 71.4 us
    pallas_call x0 -> x4, Pallas kernels: none -> 52.8 us  [the longest x1 27.5 us: per_device(): pl.pallas_call(first_kernel, grid=(heads,), in_specs=[wide(dk), wide(dk),...]
    all_to_all x0 -> x2, blocking collectives: none -> 52.6 us  [the longest x1 34.5 us: per_device(): got = lax.all_to_all(packed, 'sp', 0, 0, tiled=True)]
    another operation x5 -> x0, matrix products: 13.1 us -> none  [the longest x3 7.27 us: span_pieces(): jax.scipy.linalg.solve_triangular(system, right_side, lower=True, unit_di...]
  transfers between devices with their start and end apart: 6 -> 2, of which waited for: 5 -> 2; matrix products, arithmetic and copies ran while one was open for 19% -> 5% of each run, Pallas kernels for 0% -> 5%
where the time goes in v1:
time: 240 us; the launch traced here: 239 us
  waiting for transfers between devices  80.1 us (33%)
  Pallas kernels  52.8 us (22%)
  blocking collectives  52.6 us (22%)
  local copies, waits for them, and re-layouts  19.1 us (8%)
  matrix products  15.5 us (6%)
  between operations  14.2 us (6%)
  other arithmetic  4.42 us (2%)
    unnamed x3, waiting for transfers between devices  71.4 us
    all_to_all x1, blocking collectives, per_device(): got = lax.all_to_all(packed, 'sp', 0, 0, tiled=True)  34.5 us
    pallas_call x1, Pallas kernels, per_device(): pl.pallas_call(first_kernel, grid=(heads,), in_specs=[wide(dk), wide(dk),...  27.5 us
    all_to_all x1, blocking collectives, per_device(): lax.all_to_all(jnp.concatenate([starts, ends], axis=2), 'sp', 0, 0, tiled...  18.2 us
    unnamed x15, local copies, waits for them, and re-layouts  12.6 us
    pallas_call x1, Pallas kernels, per_device(): pl.pallas_call(last_kernel, grid=(heads,), in_specs=[wide(dk), wide(dk),...  11.8 us
    reduce_scatter x1, waiting for transfers between devices, per_device(): lax.psum_scatter(partial_hidden.astype(bf16), 'tp', scatter_dimension=0,...  8.67 us
    pallas_call x1, Pallas kernels, per_device(): pl.pallas_call(value_kernel, grid=(heads,), in_specs=[wide(dk), per_head(...  8.09 us
  transfers between devices with their start and end apart: 2, of which 2 were waited for; matrix products, arithmetic and copies ran while one was open for 5% of the time, Pallas kernels for 5%

profile of v1, /device:TPU:0, one launch (start us, length us, event | category | flops | bytes accessed | tf_op | source)
XLA Modules:
  0.0 238.7 jit_solution(3356941761108509514)
XLA Ops:
  7.2 0.0 copy-start
  7.2 0.0 reduce-scatter.7.cloned.1.call-start
  7.2 0.7 neg.16
  8.0 1.0 fusion.1
  8.9 0.8 copy.68.g
  9.8 0.6 reshape.37.row
  10.4 0.8 copy.65
  11.2 0.7 add_divide_fusion.b
  11.9 0.0 copy-done
  11.9 4.2 %convolution_convert_fusion.1.v = bf16[256,1024]{1,0:T(8,128)(2,1)} fusion(bf16[256,2048]{1,0:T(8,128)(2,1)S(1)} %copy-done, bf16[2048,1024]{1,0:T(8,128)(2,1)} %param.11), kind=kOutput, calls=%fused_computation.2 | convolution fusion | flops 1074003968 | bytes 5767168 | tf_op jit(solution)/shard_map/dot_general | solution.py:241
  16.1 27.5 %first.1 = (bf16[8,256,256]{2,1,0:T(8,128)(2,1)}, f32[8,256,256]{2,1,0:T(8,128)}, f32[8,256,128]{2,1,0:T(8,128)}, bf16[8,128,128]{2,1,0:T(8,128)(2,1)}, bf16[8,1...) custom-call(bf16[256,1024]{1,0:T(8,128)(2,1)} %q.3, bf16[256,1024]{1,0:T(8,128)(2,1)} %k.5, ...), custom_call_target="tpu_custom_call" | custom-call | tf_op jit(solution)/shard_map/first/pallas_call | solution.py:254
  43.6 0.0 copy-start.2
  43.6 1.5 fusion.24
  45.1 0.1 pad_maximum_fusion.1
  45.2 0.1 pad_maximum_fusion.2
  45.3 0.0 copy-done.2
  45.3 0.1 broadcast_in_dim.14
  45.4 0.3 pad_maximum_fusion
  45.8 34.5 %all_to_all.10 = bf16[16,128,256]{2,1,0:T(8,128)(2,1)S(1)} all-to-all(bf16[16,128,256]{2,1,0:T(8,128)(2,1)S(1)} %pad_maximum_fusion), channel_id=1, replica_groups=mesh['sp'=16,'tp'=2] {'sp'}, dimensions={0} | all-to-all | bytes 2097152 | tf_op jit(solution)/shard_map/all_to_all | solution.py:278
  80.2 0.9 slice.36.t
  81.1 1.2 fusion.22
  82.3 5.4 %scan.1 = (bf16[16,128,64]{2,1,0:T(8,128)(2,1)}, bf16[16,128,64]{2,1,0:T(8,128)(2,1)}) custom-call(bf16[16,128,128]{2,1,0:T(8,128)(2,1)} %slice.36.t, bf16[16,128,64]{2,1,0:T(8,128)(2,1)} %get-tuple-element.61.off, bf16[16,128,64]{2,1,0:T(8,128)(2,1)} %get-tuple-element.60.own), custom_call_target="tpu_custom_call" | custom-call | tf_op jit(solution)/shard_map/scan/pallas_call | solution.py:279
  87.7 1.5 pad_maximum_fusion.3
  89.2 18.2 %all_to_all.11 = bf16[16,128,128]{2,1,0:T(8,128)(2,1)S(1)} all-to-all(bf16[16,128,128]{2,1,0:T(8,128)(2,1)S(1)} %pad_maximum_fusion.3), channel_id=1, replica_groups=mesh['sp'=16,'tp'=2] {'sp'}, dimensions={0} | all-to-all | bytes 1048576 | tf_op jit(solution)/shard_map/all_to_all | solution.py:284
  107.4 0.3 copy.69
  107.8 0.8 copy.82
  108.6 8.1 %value.1 = (f32[8,256,128]{2,1,0:T(8,128)}, bf16[256,1024]{1,0:T(8,128)(2,1)}) custom-call(bf16[256,1024]{1,0:T(8,128)(2,1)} %k.5, bf16[8,256,256]{2,1,0:T(8,128)(2,1)} %get-tuple-element.22.inv, f32[8,256,128]{2,1,0:T(8,128)} %get-tuple-element.23.dw, bf16[8,128,128]{2,1,0:T(8,128)(2,1)} %bitcast.29, f32[256,8]{1,0:T(8,128)} %add_divide_fusion.b, ...), custom_call_target="tpu_custom_call" | custom-call | tf_op jit(solution)/shard_map/value/pallas_call | solution.py:288
  116.7 4.3 %convert_bitcast_fusion = bf16[2048,1024]{0,1:T(8,128)(2,1)} fusion(bf16[256,1024]{1,0:T(8,128)(2,1)} %get-tuple-element.35, bf16[256,2048]{1,0:T(8,128)(2,1)S(1)} %copy-done), kind=kOutput, calls=%fused_computation | convolution fusion | flops 1075838976 | bytes 5767168 | tf_op jit(solution)/shard_map/dot_general | solution.py:301
  121.0 6.4 %copy.79 = bf16[2048,1024]{1,0:T(8,128)(2,1)} copy(bf16[2048,1024]{0,1:T(8,128)(2,1)} %convert_bitcast_fusion) | data formatting | bytes 8388608
  127.4 0.0 copy-start.1
  127.4 0.0 reduce-scatter.7.cloned.1.call-update
  127.4 0.0 reduce-scatter.5.cloned.1.call-start
  127.5 1.0 copy-done.1
  128.5 4.4 %convolution_convert_fusion = bf16[256,2048]{1,0:T(8,128)(2,1)} fusion(bf16[256,1024]{1,0:T(8,128)(2,1)S(1)} %copy-done.1, bf16[2048,1024]{1,0:T(8,128)(2,1)} %param.11), kind=kOutput, calls=%fused_computation.1 | convolution fusion | flops 1074266112 | bytes 5767168 | tf_op jit(solution)/shard_map/dot_general | solution.py:307
  132.9 0.0 copy-start.3
  132.9 0.0 reduce-scatter.5.cloned.1.call-update
  132.9 0.9 copy.83
  133.8 11.8 %last.1 = (bf16[256,1024]{1,0:T(8,128)(2,1)}, bf16[256,1024]{1,0:T(8,128)(2,1)}, f32[256,8]{1,0:T(8,128)}, f32[256,8]{1,0:T(8,128)}, f32[8,1,256]{2,1,0:T(1,128)}) custom-call(bf16[256,1024]{1,0:T(8,128)(2,1)} %q.3, bf16[256,1024]{1,0:T(8,128)(2,1)} %k.5, bf16[256,1024]{1,0:T(8,128)(2,1)} %convolution_convert_fusion.1.v, bf16[256,1024]{1,0:T(8,128)(2,1)} %do.3, ...), custom_call_target="tpu_custom_call" | custom-call | flops 1744830464 | bytes 12582912 | tf_op jit(solution)/shard_map/last/pallas_call | solution.py:314
  145.6 1.0 subtract_multiply_fusion
  146.6 0.7 copy.77
  147.3 1.0 copy.76
  148.2 0.0 copy-done.3
  148.2 1.5 convolution_multiply_fusion
  149.8 71.4 %reduce-scatter.7.cloned.1.call-done = bf16[128,1024]{1,0:T(8,128)(2,1)} async-done(((bf16[2048,1024]{1,0:T(8,128)(2,1)}), bf16[128,1024]{1,0:T(8,128)(2,1)}) %reduce-scatter.7.cloned.1.call-update) | async-done | bytes 262160
  221.1 1.1 copy.80
  222.2 0.9 copy.78
  223.2 8.7 %reduce-scatter.5.cloned.1.call-done = bf16[128,2048]{1,0:T(8,128)(2,1)} async-done(((bf16[256,2048]{1,0:T(8,128)(2,1)}), bf16[128,2048]{1,0:T(8,128)(2,1)}) %reduce-scatter.5.cloned.1.call-update) | async-done | bytes 524304 | tf_op jit(solution)/shard_map/reduce_scatter | solution.py:310
  (2 shorter events, 0.1 us)
Async XLA Ops:
  7.2 4.7 %copy-start = (bf16[256,2048]{1,0:T(8,128)(2,1)S(1)}, bf16[256,2048]{1,0:T(8,128)(2,1)}, u32[]{:S(2)}) copy-start(bf16[256,2048]{1,0:T(8,128)(2,1)} %param.10) | copy-start | bytes 3145732
  7.2 213.9 %reduce-scatter.7.cloned.1.call-start = ((), (), s32[]{:S(2)}) async-start(), calls=%async_computation.5 | async-start | bytes 4456448
  43.6 1.7 copy-start.2
  127.4 1.0 copy-start.1
  127.4 104.4 %reduce-scatter.5.cloned.1.call-start = ((), (), s32[]{:S(2)}) async-start(), calls=%async_computation.4 | async-start | bytes 1572864 | tf_op jit(solution)/shard_map/reduce_scatter | solution.py:310
  132.9 15.3 %copy-start.3 = (f32[256,8]{0,1:T(8,128)S(1)}, f32[256,8]{0,1:T(8,128)}, u32[]{:S(2)}) copy-start(f32[256,8]{0,1:T(8,128)} %param.13) | copy-start | bytes 24580
Sparse Core Ops, SparseCore 0:
  127.6 93.5 reduce-scatter.6
  223.9 7.8 reduce-scatter.4

commit v2 on v1

--- a/solution.py
+++ b/solution.py
@@ -7,6 +7,7 @@
 from jax.experimental.pallas import tpu as pltpu
 from jax.sharding import PartitionSpec as P
 
+
 f32 = jnp.float32
 bf16 = jnp.bfloat16
 norm_floor = 16.0
@@ -36,8 +37,8 @@
     return nn(a_hi, b_hi) + (nn(a_hi, b_lo) + nn(a_lo, b_hi))
 
 
-def invert_unit_lower(low):
-    size = low.shape[0]
+def invert_unit_lower(lows):
+    size = lows[0].shape[0]
     base = min(size, 128)
     ii = lax.broadcasted_iota(jnp.int32, (base, base), 0)
     jj = lax.broadcasted_iota(jnp.int32, (base, base), 1)
@@ -46,30 +47,34 @@
     while width < base:
         masks.append((ii // (2 * width) == jj // (2 * width)) & (ii // width != jj // width))
         width *= 2
-    parts = []
-    for start in range(0, size, base):
-        block = low[start : start + base, start : start + base]
-        inverse = jnp.where(ii == jj, 1.0, 0.0) - jnp.where(masks[0], block, 0.0)
-        parts.append([block, inverse])
+    blocks = [
+        low[start : start + base, start : start + base]
+        for low in lows
+        for start in range(0, size, base)
+    ]
+    inverses = [jnp.where(ii == jj, 1.0, 0.0) - jnp.where(masks[0], a, 0.0) for a in blocks]
     for mask in masks[1:]:
-        for part in parts:
-            off = jnp.where(mask, part[0], 0.0)
-            part[1] = part[1] - nn3(part[1], nn3(off, part[1]))
-    inverses = [part[1] for part in parts]
-    while len(inverses) > 1:
-        joined = []
-        width = inverses[0].shape[0]
+        inner = [nn3(jnp.where(mask, a, 0.0), inv) for a, inv in zip(blocks, inverses)]
+        outer = [nn3(inv, mid) for inv, mid in zip(inverses, inner)]
+        inverses = [inv - out for inv, out in zip(inverses, outer)]
+    per = size // base
+    while per > 1:
+        width = size // per
+        joined, inner = [], []
+        for pair in range(0, len(inverses), 2):
+            low = lows[pair // per]
+            row = (pair % per + 1) * width
+            inner.append(nn3(low[row : row + width, row - width : row], inverses[pair]))
         for pair in range(0, len(inverses), 2):
             first, second = inverses[pair], inverses[pair + 1]
-            row = (pair + 1) * width
-            cross = low[row : row + width, row - width : row]
-            corner = -nn3(second, nn3(cross, first))
+            corner = -nn3(second, inner[pair // 2])
             top = jnp.concatenate([first, jnp.zeros_like(first)], axis=1)
             joined.append(
                 jnp.concatenate([top, jnp.concatenate([corner, second], axis=1)], axis=0)
             )
         inverses = joined
-    return inverses[0]
+        per //= 2
+    return inverses
 
 
 def unit(raw):
@@ -82,14 +87,26 @@
     return ii >= jj, ii > jj
 
 
-def first_phase(qr, kr, v, do, b, gc, gr, ge):
+def first_phase_group(inputs):
+    prepared = [first_before(*one) for one in inputs]
+    inverses = invert_unit_lower([one[0] for one in prepared])
+    return [
+        first_after(inverse, one[1], *given)
+        for inverse, one, given in zip(inverses, prepared, inputs)
+    ]
+
+
+def first_before(qr, kr, v, do, b, gc, gr, ge):
+    k = kr * unit(kr)
+    inclusive, strict = order(qr.shape[0])
+    mask = jnp.where(inclusive, jnp.exp(jnp.minimum(gc - gr, 0.0)), 0.0)
+    return jnp.where(strict, b * nt(k, k) * mask, 0.0), mask
+
+
+def first_after(inverse, mask, qr, kr, v, do, b, gc, gr, ge):
     width = qr.shape[1]
     q = qr * (unit(qr) * width ** (-0.5))
     k = kr * unit(kr)
-    inclusive, strict = order(qr.shape[0])
-    mask = jnp.where(inclusive, jnp.exp(jnp.minimum(gc - gr, 0.0)), 0.0)
-    low = jnp.where(strict, b * nt(k, k) * mask, 0.0)
-    inverse = invert_unit_lower(low)
     eg = jnp.exp(gc)
     kd = k * jnp.exp(ge - gc)
     uw = nn(inverse, jnp.concatenate([b * v, (b * eg) * k], axis=1))
@@ -105,7 +122,7 @@
     return inverse, uw, dw0, transition, offset, own
 
 
-def value_phase(kr, inverse, dw0, end, b, gc, ge):
+def value_phase(kr, inverse, dw0, end, gc, ge):
     kd = kr * (unit(kr) * jnp.exp(ge - gc))
     return tn(inverse, dw0 + nn(kd, end))
 
@@ -162,52 +179,63 @@
 
 
 def gains(g_ref, row_ref, head):
-    gr = row_ref[0]
+    gr = row_ref[...]
     return pick(g_ref, head), gr, gr[:, gr.shape[1] - 1 :]
 
 
-def first_kernel(q, k, v, do, b, g, row, inv_o, uw_o, dw_o, t_o, off_o, own_o):
-    head = pl.program_id(0)
-    gc, gr, ge = gains(g, row, head)
-    inverse, uw, dw0, transition, offset, own = first_phase(
-        q[...].astype(f32), k[...].astype(f32), v[...].astype(f32), do[...].astype(f32),
-        pick(b, head), gc, gr, ge,
-    )
-    inv_o[0] = inverse.astype(inv_o.dtype)
-    uw_o[0] = uw
-    dw_o[0] = dw0
-    t_o[0] = transition.astype(bf16)
-    off_o[0] = offset.astype(bf16)
-    own_o[0] = own.astype(bf16)
-
-
-def value_kernel(k, inv, dw, end, b, g, row, dr_o, dv_o):
-    head = pl.program_id(0)
-    gc, gr, ge = gains(g, row, head)
-    bc = pick(b, head)
-    dr = value_phase(k[...].astype(f32), inv[0], dw[0], end[0], bc, gc, ge)
-    dr_o[0] = dr
-    dv_o[...] = (bc * dr).astype(bf16)
-
-
-def last_kernel(q, k, v, do, uw, dr, start, end, b, g, row, dq_o, dk_o, db_o, gc_o, gr_o):
-    head = pl.program_id(0)
-    gc, gr, ge = gains(g, row, head)
-    dqr, dkr, db, gcol, grow = last_phase(
-        q[...].astype(f32), k[...].astype(f32), v[...].astype(f32), do[...].astype(f32),
-        uw[0], dr[0], start[0].astype(f32), end[0].astype(f32), pick(b, head), gc, gr, ge,
-    )
-    dq_o[...] = dqr.astype(bf16)
-    dk_o[...] = dkr.astype(bf16)
-
-    @pl.when(head == 0)
+def lanes(ref, i, group):
+    width = ref.shape[1] // group
+    return ref.at[:, i * width : (i + 1) * width]
+
+
+def first_kernel(group, q, k, v, do, b, g, row, inv_o, uw_o, dw_o, t_o, off_o, own_o):
+    results = []
+    for i in range(group):
+        head = pl.program_id(0) * group + i
+        gc, gr, ge = gains(g, row.at[i], head)
+        results.append(
+            [lanes(a, i, group)[...].astype(f32) for a in (q, k, v, do)]
+            + [pick(b, head), gc, gr, ge]
+        )
+    results = first_phase_group(results)
+    for i in range(group):
+        inverse, uw, dw0, transition, offset, own = results[i]
+        inv_o[i] = inverse.astype(inv_o.dtype)
+        uw_o[i] = uw
+        dw_o[i] = dw0
+        t_o[i] = transition.astype(bf16)
+        off_o[i] = offset.astype(bf16)
+        own_o[i] = own.astype(bf16)
+
+
+def value_kernel(group, k, inv, dw, end, b, g, row, dr_o, dv_o):
+    for i in range(group):
+        head = pl.program_id(0) * group + i
+        gc, _, ge = gains(g, row.at[i], head)
+        bc = pick(b, head)
+        dr = value_phase(lanes(k, i, group)[...].astype(f32), inv[i], dw[i], end[i], gc, ge)
+        dr_o[i] = dr
+        lanes(dv_o, i, group)[...] = (bc * dr).astype(bf16)
+
+
+def last_kernel(group, q, k, v, do, uw, dr, start, end, b, g, row, dq_o, dk_o, db_o, gc_o, gr_o):
+    @pl.when(pl.program_id(0) == 0)
     def _():
         db_o[...] = jnp.zeros_like(db_o)
         gc_o[...] = jnp.zeros_like(gc_o)
 
-    put(db_o, head, db)
-    put(gc_o, head, gcol)
-    gr_o[0] = grow
+    for i in range(group):
+        head = pl.program_id(0) * group + i
+        gc, gr, ge = gains(g, row.at[i], head)
+        raw = [lanes(a, i, group)[...].astype(f32) for a in (q, k, v, do)]
+        dqr, dkr, db, gcol, grow = last_phase(
+            *raw, uw[i], dr[i], start[i].astype(f32), end[i].astype(f32), pick(b, head), gc, gr, ge
+        )
+        lanes(dq_o, i, group)[...] = dqr.astype(bf16)
+        lanes(dk_o, i, group)[...] = dkr.astype(bf16)
+        put(db_o, head, db)
+        put(gc_o, head, gcol)
+        gr_o[i] = grow
 
 
 def scan_kernel(count, t, off, own, start_o, end_o):
@@ -230,12 +258,84 @@
     lax.fori_loop(0, count, step, (zero, zero))
 
 
-def per_device(queries, keys, hidden, value_weight, beta_pre, decay_pre, decay_rate, out_grad):
+def exchange(value, axis, bit):
+    count = lax.axis_size(axis)
+    return lax.ppermute(value, axis, [(i, i ^ bit) for i in range(count)])
+
+
+def bit_of(axis, bit):
+    return (lax.axis_index(axis) >> bit) & 1
+
+
+class Halving:
+    def __init__(self, hidden, grads, bits, sequence):
+        self.grads, self.sequence = grads, sequence
+        self.length, self.rows, self.count = hidden.shape[0], hidden.shape[1], 1 << bits
+        self.left = sorted(range(bits), reverse=True)
+        self.axis = 1 + self.left.index(sequence[0])
+        self.mine = bit_of("sp", sequence[0])
+        self.split = hidden.reshape((self.length,) + (2,) * bits + (self.rows // self.count,))
+        self.send = self.product(1 - self.mine).astype(bf16)
+
+    def product(self, side):
+        piece = lax.dynamic_index_in_dim(self.split, side, self.axis, False)
+        piece = piece.reshape(self.length, self.rows // 2)
+        return lax.dot_general(
+            piece, self.grads, (((0,), (0,)), ((), ())), preferred_element_type=f32
+        )
+
+    def finish(self, send):
+        left = list(self.left)
+        got = exchange(send, "sp", 1 << self.sequence[0])
+        total = self.product(self.mine) + got.astype(f32)
+        left.remove(self.sequence[0])
+        for bit in self.sequence[1:]:
+            place = left.index(bit)
+            mine = bit_of("sp", bit)
+            shaped = total.reshape(1 << place, 2, -1, total.shape[-1])
+            send = lax.dynamic_index_in_dim(shaped, 1 - mine, 1, False)
+            keep = lax.dynamic_index_in_dim(shaped, mine, 1, False)
+            got = exchange(send.astype(bf16), "sp", 1 << bit)
+            total = keep + got.astype(f32)
+            left.remove(bit)
+        return total.reshape(self.rows // self.count, -1)
+
+
+def plan_weight(hidden, grads, count):
+    bits = count.bit_length() - 1
+    low = bits // 2
+    order_a = list(range(bits))
+    order_b = order_a[:low][::-1] + order_a[low:]
+    order_c = order_a[low:] + order_a[:low]
+    width = grads.shape[1]
+    cut = max(width * 3 // 8 // 128 * 128, 1)
+    groups = [(0, cut, order_a), (cut, 2 * cut, order_b), (2 * cut, width, order_c)]
+    return [Halving(hidden, grads[:, lo:hi], bits, seq) for lo, hi, seq in groups]
+
+
+def reduce_hidden(grads, weight):
+    cores = lax.axis_size("tp")
+    assert cores == 2
+    half = grads.shape[0] // cores
+    me = lax.axis_index("tp")
+
+    def product(side):
+        rows = lax.dynamic_slice_in_dim(grads, side * half, half, 0)
+        return lax.dot_general(
+            rows, weight, (((1,), (1,)), ((), ())), preferred_element_type=f32
+        ).astype(bf16)
+
+    got = exchange(product(1 - me), "tp", 1)
+    return (product(me).astype(f32) + got.astype(f32)).astype(bf16)
+
+
+def compute(queries, keys, hidden, value_weight, beta_pre, decay_pre, decay_rate, out_grad):
     heads = decay_rate.shape[0]
     length, dk = queries.shape[0], queries.shape[1] // heads
     dv = value_weight.shape[1] // heads
     count = lax.axis_size("sp")
     parts = count // heads
+    group = 2 if heads % 2 == 0 else 1
     cols = dv // parts
 
     values = jnp.dot(hidden, value_weight, preferred_element_type=f32).astype(bf16)
@@ -245,15 +345,15 @@
     sums = jnp.dot(inclusive, log_decay, precision=lax.Precision.HIGHEST)
     sums_row = sums.T.reshape(heads, 1, length)
 
-    wide = lambda n: pl.BlockSpec((length, n), lambda h: (0, h))
-    per_head = lambda r, c: pl.BlockSpec((1, r, c), lambda h: (h, 0, 0))
+    wide = lambda n: pl.BlockSpec((length, group * n), lambda h: (0, h))
+    per_head = lambda r, c: pl.BlockSpec((group, r, c), lambda h: (h, 0, 0))
     table = pl.BlockSpec((length, heads), lambda h: (0, 0))
     shape = jax.ShapeDtypeStruct
     params = pltpu.CompilerParams(dimension_semantics=("arbitrary",))
 
     inverse, uw, dw0, transition, offset, own = pl.pallas_call(
-        first_kernel,
-        grid=(heads,),
+        functools.partial(first_kernel, group),
+        grid=(heads // group,),
         in_specs=[wide(dk), wide(dk), wide(dv), wide(dv), table, table, per_head(1, length)],
         out_specs=[
             per_head(length, length), per_head(length, dv + dk), per_head(length, dv),
@@ -286,8 +386,8 @@
     start, end = back[:, :, 0], back[:, :, 1]
 
     dr, grad_values = pl.pallas_call(
-        value_kernel,
-        grid=(heads,),
+        functools.partial(value_kernel, group),
+        grid=(heads // group,),
         in_specs=[
             wide(dk), per_head(length, length), per_head(length, dv), per_head(dk, dv),
             table, table, per_head(1, length),
@@ -298,22 +398,14 @@
         name="value",
     )(keys, inverse, dw0, end, beta, sums, sums_row)
 
-    partial_weight = lax.dot_general(
-        hidden, grad_values, (((0,), (0,)), ((), ())), preferred_element_type=f32
-    )
-    d_weight = lax.psum_scatter(
-        partial_weight.astype(bf16), "sp", scatter_dimension=0, tiled=True
-    ).astype(f32)
-    partial_hidden = lax.dot_general(
-        grad_values, value_weight, (((1,), (1,)), ((), ())), preferred_element_type=f32
-    )
-    d_hidden = lax.psum_scatter(
-        partial_hidden.astype(bf16), "tp", scatter_dimension=0, tiled=True
-    )
+    plans = plan_weight(hidden, grad_values, count)
+    sends, dr, start = lax.optimization_barrier(([plan.send for plan in plans], dr, start))
+    d_weight = jnp.concatenate([plan.finish(x) for plan, x in zip(plans, sends)], axis=1)
+    d_hidden = reduce_hidden(grad_values, value_weight)
 
     d_queries, d_keys, db, gcol, grow = pl.pallas_call(
-        last_kernel,
-        grid=(heads,),
+        functools.partial(last_kernel, group),
+        grid=(heads // group,),
         in_specs=[
             wide(dk), wide(dk), wide(dv), wide(dv), per_head(length, dv + dk),
             per_head(length, dv), per_head(dk, dv), per_head(dk, dv),
@@ -339,7 +431,7 @@
 
 def solution(mesh):
     return jax.shard_map(
-        per_device,
+        compute,
         mesh=mesh,
         in_specs=(
             P("sp", "tp"), P("sp", "tp"), P("sp", None), P(None, "tp"),

time: 240 us -> 175 us (0.73)
  waiting for transfers between devices: 80.1 us -> 44.5 us
  blocking collectives: 52.6 us -> 34.5 us
  starting transfers between devices: 0.08 us -> 17.9 us
  Pallas kernels: 52.8 us -> 38.8 us
  between operations: 14.2 us -> 0.99 us
  local copies, waits for them, and re-layouts: 19.1 us -> 13.4 us
  matrix products: 15.5 us -> 18.5 us
    unnamed x3 -> x0, waiting for transfers between devices: 71.4 us -> none
    ppermute x0 -> x13, waiting for transfers between devices: none -> 33.3 us  [exchange(): return lax.ppermute(value, axis, [(i, i ^ bit) for i in range(count)])]
    all_to_all x2 -> x1, blocking collectives: 52.6 us -> 34.5 us  [compute(): got = lax.all_to_all(packed, 'sp', 0, 0, tiled=True)]
    pallas_call x4, Pallas kernels: 52.8 us -> 38.8 us  [the longest x1 17.5 us: compute(): pl.pallas_call(functools.partial(first_kernel, group), grid=(heads // gro...]
    ppermute x0 -> x13, starting transfers between devices: none -> 13.9 us  [exchange(): return lax.ppermute(value, axis, [(i, i ^ bit) for i in range(count)])]
    all_to_all x0 -> x1, waiting for transfers between devices: none -> 11.2 us  [compute(): lax.all_to_all(jnp.concatenate([starts, ends], axis=2), 'sp', 0, 0, tiled...]
    unnamed x15 -> x27, local copies, waits for them, and re-layouts: 12.6 us -> 3.77 us
    reduce_scatter x1 -> x0, waiting for transfers between devices: 8.67 us -> none  [per_device(): lax.psum_scatter(partial_hidden.astype(bf16), 'tp', scatter_dimension=0,...]
  transfers between devices with their start and end apart: 2 -> 14, of which waited for: 2 -> 11; matrix products, arithmetic and copies ran while one was open for 5% -> 7% of each run, Pallas kernels for 5% -> 0%
where the time goes in v2:
time: 175 us
  waiting for transfers between devices  44.5 us (25%)
  Pallas kernels  38.8 us (22%)
  blocking collectives  34.5 us (20%)
  matrix products  18.5 us (11%)
  starting transfers between devices  17.9 us (10%)
  local copies, waits for them, and re-layouts  13.4 us (8%)
  other arithmetic  6.33 us (4%)
    all_to_all x1, blocking collectives, compute(): got = lax.all_to_all(packed, 'sp', 0, 0, tiled=True)  34.5 us
    ppermute x13, waiting for transfers between devices, exchange(): return lax.ppermute(value, axis, [(i, i ^ bit) for i in range(count)])  33.3 us
    pallas_call x1, Pallas kernels, compute(): pl.pallas_call(functools.partial(first_kernel, group), grid=(heads // gro...  17.5 us
    ppermute x13, starting transfers between devices, exchange(): return lax.ppermute(value, axis, [(i, i ^ bit) for i in range(count)])  13.9 us
    all_to_all x1, waiting for transfers between devices, compute(): lax.all_to_all(jnp.concatenate([starts, ends], axis=2), 'sp', 0, 0, tiled...  11.2 us
    pallas_call x1, Pallas kernels, compute(): pl.pallas_call(functools.partial(last_kernel, group), grid=(heads // grou...  10.4 us
    dot_general x2, matrix products, product(): lax.dot_general(rows, weight, (((1,), (1,)), ((), ())), preferred_element...  6.14 us
    dot_general x6, matrix products, product(): lax.dot_general(piece, self.grads, (((0,), (0,)), ((), ())), preferred_el...  6.03 us
  transfers between devices with their start and end apart: 14, of which 11 were waited for; matrix products, arithmetic and copies ran while one was open for 7% of the time, Pallas kernels for 0%

profile of v2, /device:TPU:0, one launch (start us, length us, event | category | flops | bytes accessed | tf_op | source)
XLA Modules:
  0.0 174.8 jit_solution(8647457896349640862)
XLA Ops:
  0.6 0.8 copy.71
  1.5 0.7 add_divide_fusion.b
  2.2 0.7 neg.16
  2.8 1.0 fusion.4
  3.8 0.9 copy.74.g
  4.6 0.6 reshape.132.row
  5.2 4.6 %convolution_convert_fusion.5.v = bf16[256,1024]{1,0:T(8,128)(2,1)} fusion(bf16[256,2048]{1,0:T(8,128)(2,1)} %param.10, bf16[2048,1024]{1,0:T(8,128)(2,1)} %param.11), kind=kOutput, calls=%fused_computation.8 | convolution fusion | flops 1074003968 | bytes 5767168 | tf_op jit(solution)/shard_map/dot_general | solution.py:341
  9.8 17.5 %first.1 = (bf16[8,256,256]{2,1,0:T(8,128)(2,1)}, f32[8,256,256]{2,1,0:T(8,128)}, f32[8,256,128]{2,1,0:T(8,128)}, bf16[8,128,128]{2,1,0:T(8,128)(2,1)}, bf16[8,1...) custom-call(bf16[256,1024]{1,0:T(8,128)(2,1)} %q.3, bf16[256,1024]{1,0:T(8,128)(2,1)} %k.5, ...), custom_call_target="tpu_custom_call" | custom-call | tf_op jit(solution)/shard_map/first/pallas_call | solution.py:354
  27.3 1.7 fusion.52
  29.0 0.1 pad_maximum_fusion.2
  29.1 0.1 pad_maximum_fusion.1
  29.3 0.1 broadcast_in_dim.14
  29.4 0.3 pad_maximum_fusion
  29.7 34.5 %all_to_all.10 = bf16[16,128,256]{2,1,0:T(8,128)(2,1)S(1)} all-to-all(bf16[16,128,256]{2,1,0:T(8,128)(2,1)S(1)} %pad_maximum_fusion), channel_id=1, replica_groups=mesh['sp'=16,'tp'=2] {'sp'}, dimensions={0} | all-to-all | bytes 2097152 | tf_op jit(solution)/shard_map/all_to_all | solution.py:378
  64.2 0.9 slice.48.t
  65.1 1.2 fusion.50
  66.3 5.5 %scan.1 = (bf16[16,128,64]{2,1,0:T(8,128)(2,1)}, bf16[16,128,64]{2,1,0:T(8,128)(2,1)}) custom-call(bf16[16,128,128]{2,1,0:T(8,128)(2,1)} %slice.48.t, bf16[16,128,64]{2,1,0:T(8,128)(2,1)} %get-tuple-element.77.off, bf16[16,128,64]{2,1,0:T(8,128)(2,1)} %get-tuple-element.76.own), custom_call_target="tpu_custom_call" | custom-call | tf_op jit(solution)/shard_map/scan/pallas_call | solution.py:379
  71.8 2.3 %pad_maximum_fusion.3 = bf16[16,128,128]{2,1,0:T(8,128)(2,1)} fusion(bf16[16,128,64]{2,1,0:T(8,128)(2,1)} %get-tuple-element.33, bf16[16,128,64]{2,1,0:T(8,128)(2,1)} %get-tuple-element.32), kind=kLoop, calls=%fused_computation.19 | loop fusion | flops 1048576 | bytes 1048576 | tf_op jit(solution)/shard_map/concatenate | solution.py:384
  74.0 4.0 %all-to-all-start.1 = ((bf16[16,128,128]{2,1,0:T(8,128)(2,1)}), bf16[16,128,128]{2,1,0:T(8,128)(2,1)S(1)}, u32[]{:S(2)}, u32[]{:S(2)}) async-start(bf16[16,128,128]{2,1,0:T(8,128)(2,1)} %pad_maximum_fusion.3), calls=%async_computation.1 | async-start | bytes 1048576 | tf_op jit(solution)/shard_map/all_to_all | solution.py:384
  78.0 0.5 copy.75
  78.6 0.9 constant_dynamic-slice_fusion.2
  79.4 0.9 constant_dynamic-slice_fusion.1
  80.3 0.9 constant_dynamic-slice_fusion
  81.2 11.2 %all-to-all-done.1 = bf16[16,128,128]{2,1,0:T(8,128)(2,1)S(1)} async-done(((bf16[16,128,128]{2,1,0:T(8,128)(2,1)}), bf16[16,128,128]{2,1,0:T(8,128)(2,1)S(1)}, u32[]{:S(2)}, u32[]{:S(2)}) %all-to-all-start.1) | async-done | bytes 524320 | tf_op jit(solution)/shard_map/all_to_all | solution.py:384
  92.4 0.3 copy.76
  92.8 0.9 copy.90
  93.7 5.3 %value.1 = (f32[8,256,128]{2,1,0:T(8,128)}, bf16[256,1024]{1,0:T(8,128)(2,1)}) custom-call(bf16[256,1024]{1,0:T(8,128)(2,1)} %k.5, bf16[8,256,256]{2,1,0:T(8,128)(2,1)} %get-tuple-element.27.inv, f32[8,256,128]{2,1,0:T(8,128)} %get-tuple-element.28.dw, bf16[8,128,128]{2,1,0:T(8,128)(2,1)} %bitcast.110, f32[256,8]{1,0:T(8,128)} %add_divide_fusion.b, ...), custom_call_target="tpu_custom_call" | custom-call | tf_op jit(solution)/shard_map/value/pallas_call | solution.py:388
  99.0 2.3 %convolution_convert_fusion.3 = bf16[1024,384]{1,0:T(8,128)(2,1)} fusion(bf16[256,1024]{0,1:T(8,128)(2,1)S(1)} %bitcast.101, bf16[256,1024]{1,0:T(8,128)(2,1)} %get-tuple-element.34), kind=kOutput, calls=%fused_computation.6 | convolution fusion | flops 201719808 | bytes 1507328 | tf_op jit(solution)/shard_map/dot_general | solution.py:283
  101.3 2.2 %convolution_convert_fusion.2 = bf16[1024,384]{1,0:T(8,128)(2,1)} fusion(bf16[256,1024]{0,1:T(8,128)(2,1)S(1)} %bitcast.102, bf16[256,1024]{1,0:T(8,128)(2,1)} %get-tuple-element.34), kind=kOutput, calls=%fused_computation.5 | convolution fusion | flops 201719808 | bytes 1507328 | tf_op jit(solution)/shard_map/dot_general | solution.py:283
  103.6 0.3 convolution_convert_fusion.4
  103.9 0.9 copy.91
  104.8 10.4 %last.1 = (bf16[256,1024]{1,0:T(8,128)(2,1)}, bf16[256,1024]{1,0:T(8,128)(2,1)}, f32[256,8]{1,0:T(8,128)}, f32[256,8]{1,0:T(8,128)}, f32[8,1,256]{2,1,0:T(1,128)}) custom-call(bf16[256,1024]{1,0:T(8,128)(2,1)} %q.3, bf16[256,1024]{1,0:T(8,128)(2,1)} %k.5, bf16[256,1024]{1,0:T(8,128)(2,1)} %convolution_convert_fusion.5.v, bf16[256,1024]{1,0:T(8,128)(2,1)} %do.3, ...), custom_call_target="tpu_custom_call" | custom-call | flops 1744830464 | bytes 12582912 | tf_op jit(solution)/shard_map/last/pallas_call | solution.py:406
  115.2 1.0 subtract_multiply_fusion
  116.1 0.7 copy.88
  116.8 1.0 copy.83
  117.8 1.3 collective-permute-start.9
  119.1 3.8 %convolution_convert_fusion = bf16[128,2048]{1,0:T(8,128)(2,1)S(1)} fusion(bf16[2048,1024]{1,0:T(8,128)(2,1)} %param.11, bf16[256,1024]{1,0:T(8,128)(2,1)S(1)} %copy-done.1, s32[]{:T(128)S(6)} %select_n.71), kind=kOutput, calls=%fused_computation | convolution fusion | flops 537133056 | bytes 4980740 | tf_op jit(solution)/shard_map/dot_general | solution.py:324
  123.0 0.1 collective-permute-start
  123.1 1.0 collective-permute-start.5
  124.0 0.6 collective-permute-start.1
  124.6 0.8 convolution_multiply_fusion
  125.4 3.8 %collective-permute-done.9 = bf16[1024,256]{1,0:T(8,128)(2,1)S(1)} collective-permute-done((bf16[1024,256]{1,0:T(8,128)(2,1)S(1)}, bf16[1024,256]{1,0:T(8,128)(2,1)S(1)}, u32[]{:S(2)}, u32[]{:S(2)}) %collective-permute-start.9) | collective-permute-done | bytes 524320 | tf_op jit(solution)/shard_map/ppermute | solution.py:263
  129.2 0.3 convert_add_fusion.2
  129.6 2.3 %collective-permute-start.10 = (bf16[1,512,256]{2,1,0:T(8,128)(2,1)S(1)}, bf16[1,512,256]{2,1,0:T(8,128)(2,1)S(1)}, u32[]{:S(2)}, u32[]{:S(2)}) collective-permute-start(bf16[1,512,256]{2,1,0:T(8,128)(2,1)S(1)} %fusion.6), channel_id=1, source_target_pairs={{0,16},{2,18},{4,20},{6,22},{8,24},{10,26},{12,28},{14,30},{16,0},... | collective-permute-start | bytes 786440 | tf_op jit(solution)/shard_map/ppermute | solution.py:263
  131.9 2.3 %add_convert_fusion = bf16[128,2048]{1,0:T(8,128)(2,1)} fusion(bf16[128,2048]{1,0:T(8,128)(2,1)S(1)} %collective-permute-done, bf16[2048,1024]{1,0:T(8,128)(2,1)S(1)} %copy-done, bf16[256,1024]{1,0:T(8,128)(2,1)S(1)} %copy-done.1, s32[]{:T(128)S(6)} %select_n.70), kind=kOutput, calls=%fused_computation.12 | convolution fusion | flops 538181632 | bytes 5505028 | tf_op jit(solution)/shard_map/dot_general | solution.py:324
  134.2 8.0 %collective-permute-done.10 = bf16[1,512,256]{2,1,0:T(8,128)(2,1)S(1)} collective-permute-done((bf16[1,512,256]{2,1,0:T(8,128)(2,1)S(1)}, bf16[1,512,256]{2,1,0:T(8,128)(2,1)S(1)}, u32[]{:S(2)}, u32[]{:S(2)}) %collective-permute-start.10) | collective-permute-done | bytes 262176 | tf_op jit(solution)/shard_map/ppermute | solution.py:263
  142.4 1.3 collective-permute-start.11
  143.7 0.4 convert_add_fusion
  144.2 0.9 collective-permute-start.6
  145.0 0.4 convert_add_fusion.1
  145.5 2.9 %collective-permute-done.11 = bf16[2,128,256]{2,1,0:T(8,128)(2,1)S(1)} collective-permute-done((bf16[2,128,256]{2,1,0:T(8,128)(2,1)S(1)}, bf16[2,128,256]{2,1,0:T(8,128)(2,1)S(1)}, u32[]{:S(2)}, u32[]{:S(2)}) %collective-permute-start.11) | collective-permute-done | bytes 131104 | tf_op jit(solution)/shard_map/ppermute | solution.py:263
  148.4 1.8 %collective-permute-start.12 = (bf16[1,128,256]{2,1,0:T(8,128)(2,1)S(1)}, bf16[1,128,256]{2,1,0:T(8,128)(2,1)S(1)}, u32[]{:S(2)}, u32[]{:S(2)}) collective-permute-start(bf16[1,128,256]{2,1,0:T(8,128)(2,1)S(1)} %dynamic-slice_convert_fusion.4), channel_id=1, source_target_pairs={{0,4},{2,6},{4,0},{6,2},{8,12},{10,14},{12,8},{14,10},{16,20},{18,... | collective-permute-start | bytes 196616 | tf_op jit(solution)/shard_map/ppermute | solution.py:263
  150.2 0.4 collective-permute-start.2
  150.6 2.8 %collective-permute-done.12 = bf16[1,128,256]{2,1,0:T(8,128)(2,1)S(1)} collective-permute-done((bf16[1,128,256]{2,1,0:T(8,128)(2,1)S(1)}, bf16[1,128,256]{2,1,0:T(8,128)(2,1)S(1)}, u32[]{:S(2)}, u32[]{:S(2)}) %collective-permute-start.12) | collective-permute-done | bytes 65568 | tf_op jit(solution)/shard_map/ppermute | solution.py:263
  153.5 2.4 %collective-permute-done.6 = bf16[4,128,384]{2,1,0:T(8,128)(2,1)S(1)} collective-permute-done((bf16[4,128,384]{2,1,0:T(8,128)(2,1)S(1)}, bf16[4,128,384]{2,1,0:T(8,128)(2,1)S(1)}, u32[]{:S(2)}, u32[]{:S(2)}) %collective-permute-start.6) | collective-permute-done | bytes 393248 | tf_op jit(solution)/shard_map/ppermute | solution.py:263
  156.0 2.3 %collective-permute-done.2 = bf16[4,128,384]{2,1,0:T(8,128)(2,1)S(1)} collective-permute-done((bf16[4,128,384]{2,1,0:T(8,128)(2,1)S(1)}, bf16[4,128,384]{2,1,0:T(8,128)(2,1)S(1)}, u32[]{:S(2)}, u32[]{:S(2)}) %collective-permute-start.2) | collective-permute-done | bytes 393248 | tf_op jit(solution)/shard_map/ppermute | solution.py:263
  158.5 2.4 %collective-permute-start.3 = (bf16[2,128,384]{2,1,0:T(8,128)(2,1)S(1)}, bf16[2,128,384]{2,1,0:T(8,128)(2,1)S(1)}, u32[]{:S(2)}, u32[]{:S(2)}) collective-permute-start(bf16[2,128,384]{2,1,0:T(8,128)(2,1)S(1)} %fusion.11), channel_id=1, source_target_pairs={{0,8},{2,10},{4,12},{6,14},{8,0},{10,2},{12,4},{14,6},{16,24},{18,... | collective-permute-start | bytes 589832 | tf_op jit(solution)/shard_map/ppermute | solution.py:263
  160.9 2.9 %collective-permute-done.7 = bf16[2,128,384]{2,1,0:T(8,128)(2,1)S(1)} collective-permute-done((bf16[2,128,384]{2,1,0:T(8,128)(2,1)S(1)}, bf16[2,128,384]{2,1,0:T(8,128)(2,1)S(1)}, u32[]{:S(2)}, u32[]{:S(2)}) %collective-permute-start.7) | collective-permute-done | bytes 196640 | tf_op jit(solution)/shard_map/ppermute | solution.py:263
  163.9 0.5 collective-permute-start.8
  164.4 2.9 %collective-permute-done.3 = bf16[2,128,384]{2,1,0:T(8,128)(2,1)S(1)} collective-permute-done((bf16[2,128,384]{2,1,0:T(8,128)(2,1)S(1)}, bf16[2,128,384]{2,1,0:T(8,128)(2,1)S(1)}, u32[]{:S(2)}, u32[]{:S(2)}) %collective-permute-start.3) | collective-permute-done | bytes 196640 | tf_op jit(solution)/shard_map/ppermute | solution.py:263
  167.3 1.3 collective-permute-start.4
  168.6 3.1 %collective-permute-done.8 = bf16[1,128,384]{2,1,0:T(8,128)(2,1)S(1)} collective-permute-done((bf16[1,128,384]{2,1,0:T(8,128)(2,1)S(1)}, bf16[1,128,384]{2,1,0:T(8,128)(2,1)S(1)}, u32[]{:S(2)}, u32[]{:S(2)}) %collective-permute-start.8) | collective-permute-done | bytes 98336 | tf_op jit(solution)/shard_map/ppermute | solution.py:263
  171.8 2.2 %collective-permute-done.4 = bf16[1,128,384]{2,1,0:T(8,128)(2,1)S(1)} collective-permute-done((bf16[1,128,384]{2,1,0:T(8,128)(2,1)S(1)}, bf16[1,128,384]{2,1,0:T(8,128)(2,1)S(1)}, u32[]{:S(2)}, u32[]{:S(2)}) %collective-permute-start.4) | collective-permute-done | bytes 98336 | tf_op jit(solution)/shard_map/ppermute | solution.py:263
  174.0 0.8 pad_maximum_fusion.4
  (46 shorter events, 0.8 us)
Async XLA Ops:
  27.3 1.9 %copy-start.8 = (bf16[8,128,128]{2,1,0:T(8,128)(2,1)S(1)}, bf16[8,128,128]{2,1,0:T(8,128)(2,1)}, u32[]{:S(2)}) copy-start(bf16[8,128,128]{2,1,0:T(8,128)(2,1)} %get-tuple-element.29) | copy-start | bytes 786436
  66.3 11.7 %copy-start.5 = (bf16[256,2048]{1,0:T(8,128)(2,1)S(1)}, bf16[256,2048]{1,0:T(8,128)(2,1)}, u32[]{:S(2)}) copy-start(bf16[256,2048]{1,0:T(8,128)(2,1)} %param.10) | copy-start | bytes 3145732
  74.0 18.4 %all-to-all-start.1 = ((bf16[16,128,128]{2,1,0:T(8,128)(2,1)}), bf16[16,128,128]{2,1,0:T(8,128)(2,1)S(1)}, u32[]{:S(2)}, u32[]{:S(2)}) async-start(bf16[16,128,128]{2,1,0:T(8,128)(2,1)} %pad_maximum_fusion.3), calls=%async_computation.1 | async-start | bytes 1048576 | tf_op jit(solution)/shard_map/all_to_all | solution.py:384
  99.0 4.6 %copy-start.1 = (bf16[256,1024]{1,0:T(8,128)(2,1)S(1)}, bf16[256,1024]{1,0:T(8,128)(2,1)}, u32[]{:S(2)}) copy-start(bf16[256,1024]{1,0:T(8,128)(2,1)} %get-tuple-element.34) | copy-start | bytes 1572868
  99.0 4.6 %copy-start.2 = (bf16[256,2,1,2,2,128]{0,5,4,3,2,1:T(8,128)(2,1)S(1)}, bf16[256,2,1,2,2,128]{0,5,4,3,2,1:T(8,128)(2,1)}, u32[]{:S(2)}) copy-start(bf16[256,2,1,2,2,128]{0,5,4,3,2,1:T(8,128)(2,1)} %get-tuple-element.75) | copy-start | bytes 1572868
  117.8 5.3 %copy-start.7 = (bf16[1024,384]{1,0:T(8,128)(2,1)S(1)}, bf16[1024,384]{1,0:T(8,128)(2,1)}, u32[]{:S(2)}) copy-start(bf16[1024,384]{1,0:T(8,128)(2,1)} %convolution_convert_fusion.2) | copy-start | bytes 2359300
  117.8 6.3 %copy-start.6 = (bf16[1024,384]{1,0:T(8,128)(2,1)S(1)}, bf16[1024,384]{1,0:T(8,128)(2,1)}, u32[]{:S(2)}) copy-start(bf16[1024,384]{1,0:T(8,128)(2,1)} %convolution_convert_fusion.3) | copy-start | bytes 2359300
  117.8 6.8 %copy-start.9 = (f32[256,8]{0,1:T(8,128)S(1)}, f32[256,8]{0,1:T(8,128)}, u32[]{:S(2)}) copy-start(f32[256,8]{0,1:T(8,128)} %param.13) | copy-start | bytes 24580
  117.8 6.8 %copy-start.10 = (f32[8,1,256]{2,1,0:T(1,128)S(1)}, f32[8,1,256]{2,1,0:T(1,128)}, u32[]{:S(2)}) copy-start(f32[8,1,256]{2,1,0:T(1,128)} %get-tuple-element.42) | copy-start | bytes 24580
  117.8 11.5 %collective-permute-start.9 = (bf16[1024,256]{1,0:T(8,128)(2,1)S(1)}, bf16[1024,256]{1,0:T(8,128)(2,1)S(1)}, u32[]{:S(2)}, u32[]{:S(2)}) collective-permute-start(bf16[1024,256]{1,0:T(8,128)(2,1)S(1)} %convolution_convert_fusion.4), channel_id=1, source_target_pairs={{0,8},{2,10},{4,12},{6,14},{8,0},{10,2},{12,4},{14,6},{16,24},{18,... | collective-permute-start | bytes 1572872 | tf_op jit(solution)/shard_map/ppermute | solution.py:263
  119.1 12.8 %copy-start = (bf16[2048,1024]{1,0:T(8,128)(2,1)S(1)}, bf16[2048,1024]{1,0:T(8,128)(2,1)}, u32[]{:S(2)}) copy-start(bf16[2048,1024]{1,0:T(8,128)(2,1)} %param.11) | copy-start | bytes 12582916
  123.0 9.0 %collective-permute-start = (bf16[128,2048]{1,0:T(8,128)(2,1)S(1)}, bf16[128,2048]{1,0:T(8,128)(2,1)S(1)}, u32[]{:S(2)}, u32[]{:S(2)}) collective-permute-start(bf16[128,2048]{1,0:T(8,128)(2,1)S(1)} %convolution_convert_fusion), channel_id=1, source_target_pairs={{0,1},{1,0},{2,3},{3,2},{4,5},{5,4},{6,7},{7,6},{8,9},{9,8},{10,11... | collective-permute-start | bytes 1572872 | tf_op jit(solution)/shard_map/ppermute | solution.py:263
  123.1 20.6 %collective-permute-start.5 = (bf16[1024,384]{1,0:T(8,128)(2,1)S(1)}, bf16[1024,384]{1,0:T(8,128)(2,1)S(1)}, u32[]{:S(2)}, u32[]{:S(2)}) collective-permute-start(bf16[1024,384]{1,0:T(8,128)(2,1)S(1)} %copy-done.7), channel_id=1, source_target_pairs={{0,4},{2,6},{4,0},{6,2},{8,12},{10,14},{12,8},{14,10},{16,20},{18,... | collective-permute-start | bytes 2359304 | tf_op jit(solution)/shard_map/ppermute | solution.py:263
  124.0 21.0 %collective-permute-start.1 = (bf16[1024,384]{1,0:T(8,128)(2,1)S(1)}, bf16[1024,384]{1,0:T(8,128)(2,1)S(1)}, u32[]{:S(2)}, u32[]{:S(2)}) collective-permute-start(bf16[1024,384]{1,0:T(8,128)(2,1)S(1)} %copy-done.6), channel_id=1, source_target_pairs={{0,2},{2,0},{4,6},{6,4},{8,10},{10,8},{12,14},{14,12},{16,18},{18,... | collective-permute-start | bytes 2359304 | tf_op jit(solution)/shard_map/ppermute | solution.py:263
  129.6 14.1 %copy-start.4 = (bf16[256,2,2,1,2,128]{0,5,4,3,2,1:T(8,128)(2,1)S(1)}, bf16[256,2,2,1,2,128]{0,5,4,3,2,1:T(8,128)(2,1)}, u32[]{:S(2)}) copy-start(bf16[256,2,2,1,2,128]{0,5,4,3,2,1:T(8,128)(2,1)} %get-tuple-element.72) | copy-start | bytes 1572868
  129.6 12.7 %collective-permute-start.10 = (bf16[1,512,256]{2,1,0:T(8,128)(2,1)S(1)}, bf16[1,512,256]{2,1,0:T(8,128)(2,1)S(1)}, u32[]{:S(2)}, u32[]{:S(2)}) collective-permute-start(bf16[1,512,256]{2,1,0:T(8,128)(2,1)S(1)} %fusion.6), channel_id=1, source_target_pairs={{0,16},{2,18},{4,20},{6,22},{8,24},{10,26},{12,28},{14,30},{16,0},... | collective-permute-start | bytes 786440 | tf_op jit(solution)/shard_map/ppermute | solution.py:263
  142.3 2.7 %copy-start.3 = (bf16[256,2,2,2,1,128]{0,5,4,3,2,1:T(8,128)(2,1)S(1)}, bf16[256,2,2,2,1,128]{0,5,4,3,2,1:T(8,128)(2,1)}, u32[]{:S(2)}) copy-start(bf16[256,2,2,2,1,128]{0,5,4,3,2,1:T(8,128)(2,1)} %get-tuple-element.70) | copy-start | bytes 1572868
  142.4 6.0 %collective-permute-start.11 = (bf16[2,128,256]{2,1,0:T(8,128)(2,1)S(1)}, bf16[2,128,256]{2,1,0:T(8,128)(2,1)S(1)}, u32[]{:S(2)}, u32[]{:S(2)}) collective-permute-start(bf16[2,128,256]{2,1,0:T(8,128)(2,1)S(1)} %fusion.23), channel_id=1, source_target_pairs={{0,2},{2,0},{4,6},{6,4},{8,10},{10,8},{12,14},{14,12},{16,18},{18,... | collective-permute-start | bytes 393224 | tf_op jit(solution)/shard_map/ppermute | solution.py:263
  144.2 11.7 %collective-permute-start.6 = (bf16[4,128,384]{2,1,0:T(8,128)(2,1)S(1)}, bf16[4,128,384]{2,1,0:T(8,128)(2,1)S(1)}, u32[]{:S(2)}, u32[]{:S(2)}) collective-permute-start(bf16[4,128,384]{2,1,0:T(8,128)(2,1)S(1)} %fusion.1), channel_id=1, source_target_pairs={{0,2},{2,0},{4,6},{6,4},{8,10},{10,8},{12,14},{14,12},{16,18},{18,... | collective-permute-start | bytes 1179656 | tf_op jit(solution)/shard_map/ppermute | solution.py:263
  148.4 5.0 %collective-permute-start.12 = (bf16[1,128,256]{2,1,0:T(8,128)(2,1)S(1)}, bf16[1,128,256]{2,1,0:T(8,128)(2,1)S(1)}, u32[]{:S(2)}, u32[]{:S(2)}) collective-permute-start(bf16[1,128,256]{2,1,0:T(8,128)(2,1)S(1)} %dynamic-slice_convert_fusion.4), channel_id=1, source_target_pairs={{0,4},{2,6},{4,0},{6,2},{8,12},{10,14},{12,8},{14,10},{16,20},{18,... | collective-permute-start | bytes 196616 | tf_op jit(solution)/shard_map/ppermute | solution.py:263
  150.2 8.1 %collective-permute-start.2 = (bf16[4,128,384]{2,1,0:T(8,128)(2,1)S(1)}, bf16[4,128,384]{2,1,0:T(8,128)(2,1)S(1)}, u32[]{:S(2)}, u32[]{:S(2)}) collective-permute-start(bf16[4,128,384]{2,1,0:T(8,128)(2,1)S(1)} %fusion.2), channel_id=1, source_target_pairs={{0,4},{2,6},{4,0},{6,2},{8,12},{10,14},{12,8},{14,10},{16,20},{18,... | collective-permute-start | bytes 1179656 | tf_op jit(solution)/shard_map/ppermute | solution.py:263
  155.9 7.8 %collective-permute-start.7 = (bf16[2,128,384]{2,1,0:T(8,128)(2,1)S(1)}, bf16[2,128,384]{2,1,0:T(8,128)(2,1)S(1)}, u32[]{:S(2)}, u32[]{:S(2)}) collective-permute-start(bf16[2,128,384]{2,1,0:T(8,128)(2,1)S(1)} %fusion.12), channel_id=1, source_target_pairs={{0,8},{2,10},{4,12},{6,14},{8,0},{10,2},{12,4},{14,6},{16,24},{18,... | collective-permute-start | bytes 589832 | tf_op jit(solution)/shard_map/ppermute | solution.py:263
  158.5 8.8 %collective-permute-start.3 = (bf16[2,128,384]{2,1,0:T(8,128)(2,1)S(1)}, bf16[2,128,384]{2,1,0:T(8,128)(2,1)S(1)}, u32[]{:S(2)}, u32[]{:S(2)}) collective-permute-start(bf16[2,128,384]{2,1,0:T(8,128)(2,1)S(1)} %fusion.11), channel_id=1, source_target_pairs={{0,8},{2,10},{4,12},{6,14},{8,0},{10,2},{12,4},{14,6},{16,24},{18,... | collective-permute-start | bytes 589832 | tf_op jit(solution)/shard_map/ppermute | solution.py:263
  163.9 7.9 %collective-permute-start.8 = (bf16[1,128,384]{2,1,0:T(8,128)(2,1)S(1)}, bf16[1,128,384]{2,1,0:T(8,128)(2,1)S(1)}, u32[]{:S(2)}, u32[]{:S(2)}) collective-permute-start(bf16[1,128,384]{2,1,0:T(8,128)(2,1)S(1)} %dynamic-slice_convert_fusion.2), channel_id=1, source_target_pairs={{0,16},{2,18},{4,20},{6,22},{8,24},{10,26},{12,28},{14,30},{16,0},... | collective-permute-start | bytes 294920 | tf_op jit(solution)/shard_map/ppermute | solution.py:263
  167.3 6.6 %collective-permute-start.4 = (bf16[1,128,384]{2,1,0:T(8,128)(2,1)S(1)}, bf16[1,128,384]{2,1,0:T(8,128)(2,1)S(1)}, u32[]{:S(2)}, u32[]{:S(2)}) collective-permute-start(bf16[1,128,384]{2,1,0:T(8,128)(2,1)S(1)} %dynamic-slice_convert_fusion.3), channel_id=1, source_target_pairs={{0,16},{2,18},{4,20},{6,22},{8,24},{10,26},{12,28},{14,30},{16,0},... | collective-permute-start | bytes 294920 | tf_op jit(solution)/shard_map/ppermute | solution.py:263

commit v3 on v2

--- a/solution.py
+++ b/solution.py
@@ -325,7 +325,8 @@
             rows, weight, (((1,), (1,)), ((), ())), preferred_element_type=f32
         ).astype(bf16)
 
-    got = exchange(product(1 - me), "tp", 1)
+    send = product(1 - me)
+    got = exchange(send, "tp", 1)
     return (product(me).astype(f32) + got.astype(f32)).astype(bf16)
 
 
@@ -335,7 +336,7 @@
     dv = value_weight.shape[1] // heads
     count = lax.axis_size("sp")
     parts = count // heads
-    group = 2 if heads % 2 == 0 else 1
+    group = 4 if heads % 4 == 0 else 1
     cols = dv // parts
 
     values = jnp.dot(hidden, value_weight, preferred_element_type=f32).astype(bf16)

time: 175 us -> 170 us (0.971)
  Pallas kernels: 38.8 us -> 33.6 us
    pallas_call x1, Pallas kernels: 17.5 us -> 13.6 us  [compute(): pl.pallas_call(functools.partial(first_kernel, group), grid=(heads // gro...]
where the time goes in v3:
time: 170 us
  waiting for transfers between devices  44.6 us (26%)
  blocking collectives  34.5 us (20%)
  Pallas kernels  33.6 us (20%)
  matrix products  18.5 us (11%)
  starting transfers between devices  17.8 us (10%)
  local copies, waits for them, and re-layouts  13.4 us (8%)
  other arithmetic  6.33 us (4%)
    all_to_all x1, blocking collectives, compute(): got = lax.all_to_all(packed, 'sp', 0, 0, tiled=True)  34.5 us
    ppermute x13, waiting for transfers between devices, exchange(): return lax.ppermute(value, axis, [(i, i ^ bit) for i in range(count)])  33.4 us
    ppermute x13, starting transfers between devices, exchange(): return lax.ppermute(value, axis, [(i, i ^ bit) for i in range(count)])  13.8 us
    pallas_call x1, Pallas kernels, compute(): pl.pallas_call(functools.partial(first_kernel, group), grid=(heads // gro...  13.6 us
    all_to_all x1, waiting for transfers between devices, compute(): lax.all_to_all(jnp.concatenate([starts, ends], axis=2), 'sp', 0, 0, tiled...  11.2 us
    pallas_call x1, Pallas kernels, compute(): pl.pallas_call(functools.partial(last_kernel, group), grid=(heads // grou...  9.85 us
    dot_general x2, matrix products, product(): lax.dot_general(rows, weight, (((1,), (1,)), ((), ())), preferred_element...  6.14 us
    dot_general x6, matrix products, product(): lax.dot_general(piece, self.grads, (((0,), (0,)), ((), ())), preferred_el...  6.04 us
  transfers between devices with their start and end apart: 14, of which 11 were waited for; matrix products, arithmetic and copies ran while one was open for 7% of the time, Pallas kernels for 0%

profile of v3, /device:TPU:0, one launch (start us, length us, event | category | flops | bytes accessed | tf_op | source)
XLA Modules:
  0.0 169.6 jit_solution(9985640826320211733)
XLA Ops:
  0.6 0.8 copy.71
  1.5 0.7 add_divide_fusion.b
  2.2 0.7 neg.16
  2.8 1.0 fusion.4
  3.8 0.9 copy.74.g
  4.6 0.6 reshape.132.row
  5.2 4.6 %convolution_convert_fusion.5.v = bf16[256,1024]{1,0:T(8,128)(2,1)} fusion(bf16[256,2048]{1,0:T(8,128)(2,1)} %param.10, bf16[2048,1024]{1,0:T(8,128)(2,1)} %param.11), kind=kOutput, calls=%fused_computation.8 | convolution fusion | flops 1074003968 | bytes 5767168 | tf_op jit(solution)/shard_map/dot_general | solution.py:342
  9.8 13.6 %first.1 = (bf16[8,256,256]{2,1,0:T(8,128)(2,1)}, f32[8,256,256]{2,1,0:T(8,128)}, f32[8,256,128]{2,1,0:T(8,128)}, bf16[8,128,128]{2,1,0:T(8,128)(2,1)}, bf16[8,1...) custom-call(bf16[256,1024]{1,0:T(8,128)(2,1)} %q.3, bf16[256,1024]{1,0:T(8,128)(2,1)} %k.5, ...), custom_call_target="tpu_custom_call" | custom-call | tf_op jit(solution)/shard_map/first/pallas_call | solution.py:355
  23.4 1.7 fusion.52
  25.1 0.1 pad_maximum_fusion.2
  25.2 0.1 pad_maximum_fusion.1
  25.3 0.1 broadcast_in_dim.14
  25.4 0.3 pad_maximum_fusion
  25.7 34.5 %all_to_all.10 = bf16[16,128,256]{2,1,0:T(8,128)(2,1)S(1)} all-to-all(bf16[16,128,256]{2,1,0:T(8,128)(2,1)S(1)} %pad_maximum_fusion), channel_id=1, replica_groups=mesh['sp'=16,'tp'=2] {'sp'}, dimensions={0} | all-to-all | bytes 2097152 | tf_op jit(solution)/shard_map/all_to_all | solution.py:379
  60.2 0.9 slice.48.t
  61.1 1.2 fusion.50
  62.3 5.5 %scan.1 = (bf16[16,128,64]{2,1,0:T(8,128)(2,1)}, bf16[16,128,64]{2,1,0:T(8,128)(2,1)}) custom-call(bf16[16,128,128]{2,1,0:T(8,128)(2,1)} %slice.48.t, bf16[16,128,64]{2,1,0:T(8,128)(2,1)} %get-tuple-element.77.off, bf16[16,128,64]{2,1,0:T(8,128)(2,1)} %get-tuple-element.76.own), custom_call_target="tpu_custom_call" | custom-call | tf_op jit(solution)/shard_map/scan/pallas_call | solution.py:380
  67.8 2.3 %pad_maximum_fusion.3 = bf16[16,128,128]{2,1,0:T(8,128)(2,1)} fusion(bf16[16,128,64]{2,1,0:T(8,128)(2,1)} %get-tuple-element.33, bf16[16,128,64]{2,1,0:T(8,128)(2,1)} %get-tuple-element.32), kind=kLoop, calls=%fused_computation.19 | loop fusion | flops 1048576 | bytes 1048576 | tf_op jit(solution)/shard_map/concatenate | solution.py:385
  70.1 4.0 %all-to-all-start.1 = ((bf16[16,128,128]{2,1,0:T(8,128)(2,1)}), bf16[16,128,128]{2,1,0:T(8,128)(2,1)S(1)}, u32[]{:S(2)}, u32[]{:S(2)}) async-start(bf16[16,128,128]{2,1,0:T(8,128)(2,1)} %pad_maximum_fusion.3), calls=%async_computation.1 | async-start | bytes 1048576 | tf_op jit(solution)/shard_map/all_to_all | solution.py:385
  74.1 0.5 copy.75
  74.6 0.9 constant_dynamic-slice_fusion.2
  75.5 0.9 constant_dynamic-slice_fusion.1
  76.4 0.9 constant_dynamic-slice_fusion
  77.3 11.2 %all-to-all-done.1 = bf16[16,128,128]{2,1,0:T(8,128)(2,1)S(1)} async-done(((bf16[16,128,128]{2,1,0:T(8,128)(2,1)}), bf16[16,128,128]{2,1,0:T(8,128)(2,1)S(1)}, u32[]{:S(2)}, u32[]{:S(2)}) %all-to-all-start.1) | async-done | bytes 524320 | tf_op jit(solution)/shard_map/all_to_all | solution.py:385
  88.5 0.3 copy.76
  88.8 0.9 copy.90
  89.7 4.7 %value.1 = (f32[8,256,128]{2,1,0:T(8,128)}, bf16[256,1024]{1,0:T(8,128)(2,1)}) custom-call(bf16[256,1024]{1,0:T(8,128)(2,1)} %k.5, bf16[8,256,256]{2,1,0:T(8,128)(2,1)} %get-tuple-element.27.inv, f32[8,256,128]{2,1,0:T(8,128)} %get-tuple-element.28.dw, bf16[8,128,128]{2,1,0:T(8,128)(2,1)} %bitcast.110, f32[256,8]{1,0:T(8,128)} %add_divide_fusion.b, ...), custom_call_target="tpu_custom_call" | custom-call | tf_op jit(solution)/shard_map/value/pallas_call | solution.py:389
  94.4 2.3 %convolution_convert_fusion.3 = bf16[1024,384]{1,0:T(8,128)(2,1)} fusion(bf16[256,1024]{0,1:T(8,128)(2,1)S(1)} %bitcast.101, bf16[256,1024]{1,0:T(8,128)(2,1)} %get-tuple-element.34), kind=kOutput, calls=%fused_computation.6 | convolution fusion | flops 201719808 | bytes 1507328 | tf_op jit(solution)/shard_map/dot_general | solution.py:283
  96.7 2.3 %convolution_convert_fusion.2 = bf16[1024,384]{1,0:T(8,128)(2,1)} fusion(bf16[256,1024]{0,1:T(8,128)(2,1)S(1)} %bitcast.102, bf16[256,1024]{1,0:T(8,128)(2,1)} %get-tuple-element.34), kind=kOutput, calls=%fused_computation.5 | convolution fusion | flops 201719808 | bytes 1507328 | tf_op jit(solution)/shard_map/dot_general | solution.py:283
  99.0 0.3 convolution_convert_fusion.4
  99.3 0.9 copy.91
  100.1 9.8 %last.1 = (bf16[256,1024]{1,0:T(8,128)(2,1)}, bf16[256,1024]{1,0:T(8,128)(2,1)}, f32[256,8]{1,0:T(8,128)}, f32[256,8]{1,0:T(8,128)}, f32[8,1,256]{2,1,0:T(1,128)}) custom-call(bf16[256,1024]{1,0:T(8,128)(2,1)} %q.3, bf16[256,1024]{1,0:T(8,128)(2,1)} %k.5, bf16[256,1024]{1,0:T(8,128)(2,1)} %convolution_convert_fusion.5.v, bf16[256,1024]{1,0:T(8,128)(2,1)} %do.3, ...), custom_call_target="tpu_custom_call" | custom-call | flops 1744830464 | bytes 12582912 | tf_op jit(solution)/shard_map/last/pallas_call | solution.py:407
  110.0 1.0 subtract_multiply_fusion
  110.9 0.7 copy.88
  111.6 1.0 copy.83
  112.6 1.3 collective-permute-start.9
  113.9 3.8 %convolution_convert_fusion = bf16[128,2048]{1,0:T(8,128)(2,1)S(1)} fusion(bf16[2048,1024]{1,0:T(8,128)(2,1)} %param.11, bf16[256,1024]{1,0:T(8,128)(2,1)S(1)} %copy-done.1, s32[]{:T(128)S(6)} %select_n.71), kind=kOutput, calls=%fused_computation | convolution fusion | flops 537133056 | bytes 4980740 | tf_op jit(solution)/shard_map/dot_general | solution.py:324
  117.8 0.1 collective-permute-start
  117.8 1.0 collective-permute-start.5
  118.8 0.6 collective-permute-start.1
  119.4 0.8 convolution_multiply_fusion
  120.2 3.8 %collective-permute-done.9 = bf16[1024,256]{1,0:T(8,128)(2,1)S(1)} collective-permute-done((bf16[1024,256]{1,0:T(8,128)(2,1)S(1)}, bf16[1024,256]{1,0:T(8,128)(2,1)S(1)}, u32[]{:S(2)}, u32[]{:S(2)}) %collective-permute-start.9) | collective-permute-done | bytes 524320 | tf_op jit(solution)/shard_map/ppermute | solution.py:263
  124.0 0.3 convert_add_fusion.2
  124.4 2.4 %collective-permute-start.10 = (bf16[1,512,256]{2,1,0:T(8,128)(2,1)S(1)}, bf16[1,512,256]{2,1,0:T(8,128)(2,1)S(1)}, u32[]{:S(2)}, u32[]{:S(2)}) collective-permute-start(bf16[1,512,256]{2,1,0:T(8,128)(2,1)S(1)} %fusion.6), channel_id=1, source_target_pairs={{0,16},{2,18},{4,20},{6,22},{8,24},{10,26},{12,28},{14,30},{16,0},... | collective-permute-start | bytes 786440 | tf_op jit(solution)/shard_map/ppermute | solution.py:263
  126.8 2.3 %add_convert_fusion = bf16[128,2048]{1,0:T(8,128)(2,1)} fusion(bf16[128,2048]{1,0:T(8,128)(2,1)S(1)} %collective-permute-done, bf16[2048,1024]{1,0:T(8,128)(2,1)S(1)} %copy-done, bf16[256,1024]{1,0:T(8,128)(2,1)S(1)} %copy-done.1, s32[]{:T(128)S(6)} %select_n.70), kind=kOutput, calls=%fused_computation.12 | convolution fusion | flops 538181632 | bytes 5505028 | tf_op jit(solution)/shard_map/dot_general | solution.py:324
  129.1 8.0 %collective-permute-done.10 = bf16[1,512,256]{2,1,0:T(8,128)(2,1)S(1)} collective-permute-done((bf16[1,512,256]{2,1,0:T(8,128)(2,1)S(1)}, bf16[1,512,256]{2,1,0:T(8,128)(2,1)S(1)}, u32[]{:S(2)}, u32[]{:S(2)}) %collective-permute-start.10) | collective-permute-done | bytes 262176 | tf_op jit(solution)/shard_map/ppermute | solution.py:263
  137.2 1.3 collective-permute-start.11
  138.5 0.4 convert_add_fusion
  139.0 0.9 collective-permute-start.6
  139.8 0.4 convert_add_fusion.1
  140.3 2.9 %collective-permute-done.11 = bf16[2,128,256]{2,1,0:T(8,128)(2,1)S(1)} collective-permute-done((bf16[2,128,256]{2,1,0:T(8,128)(2,1)S(1)}, bf16[2,128,256]{2,1,0:T(8,128)(2,1)S(1)}, u32[]{:S(2)}, u32[]{:S(2)}) %collective-permute-start.11) | collective-permute-done | bytes 131104 | tf_op jit(solution)/shard_map/ppermute | solution.py:263
  143.2 1.8 %collective-permute-start.12 = (bf16[1,128,256]{2,1,0:T(8,128)(2,1)S(1)}, bf16[1,128,256]{2,1,0:T(8,128)(2,1)S(1)}, u32[]{:S(2)}, u32[]{:S(2)}) collective-permute-start(bf16[1,128,256]{2,1,0:T(8,128)(2,1)S(1)} %dynamic-slice_convert_fusion.4), channel_id=1, source_target_pairs={{0,4},{2,6},{4,0},{6,2},{8,12},{10,14},{12,8},{14,10},{16,20},{18,... | collective-permute-start | bytes 196616 | tf_op jit(solution)/shard_map/ppermute | solution.py:263
  145.0 0.4 collective-permute-start.2
  145.4 2.8 %collective-permute-done.12 = bf16[1,128,256]{2,1,0:T(8,128)(2,1)S(1)} collective-permute-done((bf16[1,128,256]{2,1,0:T(8,128)(2,1)S(1)}, bf16[1,128,256]{2,1,0:T(8,128)(2,1)S(1)}, u32[]{:S(2)}, u32[]{:S(2)}) %collective-permute-start.12) | collective-permute-done | bytes 65568 | tf_op jit(solution)/shard_map/ppermute | solution.py:263
  148.3 2.4 %collective-permute-done.6 = bf16[4,128,384]{2,1,0:T(8,128)(2,1)S(1)} collective-permute-done((bf16[4,128,384]{2,1,0:T(8,128)(2,1)S(1)}, bf16[4,128,384]{2,1,0:T(8,128)(2,1)S(1)}, u32[]{:S(2)}, u32[]{:S(2)}) %collective-permute-start.6) | collective-permute-done | bytes 393248 | tf_op jit(solution)/shard_map/ppermute | solution.py:263
  150.8 2.3 %collective-permute-done.2 = bf16[4,128,384]{2,1,0:T(8,128)(2,1)S(1)} collective-permute-done((bf16[4,128,384]{2,1,0:T(8,128)(2,1)S(1)}, bf16[4,128,384]{2,1,0:T(8,128)(2,1)S(1)}, u32[]{:S(2)}, u32[]{:S(2)}) %collective-permute-start.2) | collective-permute-done | bytes 393248 | tf_op jit(solution)/shard_map/ppermute | solution.py:263
  153.3 2.4 %collective-permute-start.3 = (bf16[2,128,384]{2,1,0:T(8,128)(2,1)S(1)}, bf16[2,128,384]{2,1,0:T(8,128)(2,1)S(1)}, u32[]{:S(2)}, u32[]{:S(2)}) collective-permute-start(bf16[2,128,384]{2,1,0:T(8,128)(2,1)S(1)} %fusion.11), channel_id=1, source_target_pairs={{0,8},{2,10},{4,12},{6,14},{8,0},{10,2},{12,4},{14,6},{16,24},{18,... | collective-permute-start | bytes 589832 | tf_op jit(solution)/shard_map/ppermute | solution.py:263
  155.6 2.9 %collective-permute-done.7 = bf16[2,128,384]{2,1,0:T(8,128)(2,1)S(1)} collective-permute-done((bf16[2,128,384]{2,1,0:T(8,128)(2,1)S(1)}, bf16[2,128,384]{2,1,0:T(8,128)(2,1)S(1)}, u32[]{:S(2)}, u32[]{:S(2)}) %collective-permute-start.7) | collective-permute-done | bytes 196640 | tf_op jit(solution)/shard_map/ppermute | solution.py:263
  158.7 0.5 collective-permute-start.8
  159.2 2.9 %collective-permute-done.3 = bf16[2,128,384]{2,1,0:T(8,128)(2,1)S(1)} collective-permute-done((bf16[2,128,384]{2,1,0:T(8,128)(2,1)S(1)}, bf16[2,128,384]{2,1,0:T(8,128)(2,1)S(1)}, u32[]{:S(2)}, u32[]{:S(2)}) %collective-permute-start.3) | collective-permute-done | bytes 196640 | tf_op jit(solution)/shard_map/ppermute | solution.py:263
  162.1 1.3 collective-permute-start.4
  163.4 3.1 %collective-permute-done.8 = bf16[1,128,384]{2,1,0:T(8,128)(2,1)S(1)} collective-permute-done((bf16[1,128,384]{2,1,0:T(8,128)(2,1)S(1)}, bf16[1,128,384]{2,1,0:T(8,128)(2,1)S(1)}, u32[]{:S(2)}, u32[]{:S(2)}) %collective-permute-start.8) | collective-permute-done | bytes 98336 | tf_op jit(solution)/shard_map/ppermute | solution.py:263
  166.6 2.2 %collective-permute-done.4 = bf16[1,128,384]{2,1,0:T(8,128)(2,1)S(1)} collective-permute-done((bf16[1,128,384]{2,1,0:T(8,128)(2,1)S(1)}, bf16[1,128,384]{2,1,0:T(8,128)(2,1)S(1)}, u32[]{:S(2)}, u32[]{:S(2)}) %collective-permute-start.4) | collective-permute-done | bytes 98336 | tf_op jit(solution)/shard_map/ppermute | solution.py:263
  168.8 0.8 pad_maximum_fusion.4
  (46 shorter events, 0.8 us)
Async XLA Ops:
  23.4 1.9 %copy-start.8 = (bf16[8,128,128]{2,1,0:T(8,128)(2,1)S(1)}, bf16[8,128,128]{2,1,0:T(8,128)(2,1)}, u32[]{:S(2)}) copy-start(bf16[8,128,128]{2,1,0:T(8,128)(2,1)} %get-tuple-element.29) | copy-start | bytes 786436
  62.3 11.7 %copy-start.5 = (bf16[256,2048]{1,0:T(8,128)(2,1)S(1)}, bf16[256,2048]{1,0:T(8,128)(2,1)}, u32[]{:S(2)}) copy-start(bf16[256,2048]{1,0:T(8,128)(2,1)} %param.10) | copy-start | bytes 3145732
  70.1 18.4 %all-to-all-start.1 = ((bf16[16,128,128]{2,1,0:T(8,128)(2,1)}), bf16[16,128,128]{2,1,0:T(8,128)(2,1)S(1)}, u32[]{:S(2)}, u32[]{:S(2)}) async-start(bf16[16,128,128]{2,1,0:T(8,128)(2,1)} %pad_maximum_fusion.3), calls=%async_computation.1 | async-start | bytes 1048576 | tf_op jit(solution)/shard_map/all_to_all | solution.py:385
  94.4 4.6 %copy-start.1 = (bf16[256,1024]{1,0:T(8,128)(2,1)S(1)}, bf16[256,1024]{1,0:T(8,128)(2,1)}, u32[]{:S(2)}) copy-start(bf16[256,1024]{1,0:T(8,128)(2,1)} %get-tuple-element.34) | copy-start | bytes 1572868
  94.4 4.6 %copy-start.2 = (bf16[256,2,1,2,2,128]{0,5,4,3,2,1:T(8,128)(2,1)S(1)}, bf16[256,2,1,2,2,128]{0,5,4,3,2,1:T(8,128)(2,1)}, u32[]{:S(2)}) copy-start(bf16[256,2,1,2,2,128]{0,5,4,3,2,1:T(8,128)(2,1)} %get-tuple-element.75) | copy-start | bytes 1572868
  112.5 5.3 %copy-start.7 = (bf16[1024,384]{1,0:T(8,128)(2,1)S(1)}, bf16[1024,384]{1,0:T(8,128)(2,1)}, u32[]{:S(2)}) copy-start(bf16[1024,384]{1,0:T(8,128)(2,1)} %convolution_convert_fusion.2) | copy-start | bytes 2359300
  112.6 6.3 %copy-start.6 = (bf16[1024,384]{1,0:T(8,128)(2,1)S(1)}, bf16[1024,384]{1,0:T(8,128)(2,1)}, u32[]{:S(2)}) copy-start(bf16[1024,384]{1,0:T(8,128)(2,1)} %convolution_convert_fusion.3) | copy-start | bytes 2359300
  112.6 6.8 %copy-start.9 = (f32[256,8]{0,1:T(8,128)S(1)}, f32[256,8]{0,1:T(8,128)}, u32[]{:S(2)}) copy-start(f32[256,8]{0,1:T(8,128)} %param.13) | copy-start | bytes 24580
  112.6 6.8 %copy-start.10 = (f32[8,1,256]{2,1,0:T(1,128)S(1)}, f32[8,1,256]{2,1,0:T(1,128)}, u32[]{:S(2)}) copy-start(f32[8,1,256]{2,1,0:T(1,128)} %get-tuple-element.42) | copy-start | bytes 24580
  112.6 11.5 %collective-permute-start.9 = (bf16[1024,256]{1,0:T(8,128)(2,1)S(1)}, bf16[1024,256]{1,0:T(8,128)(2,1)S(1)}, u32[]{:S(2)}, u32[]{:S(2)}) collective-permute-start(bf16[1024,256]{1,0:T(8,128)(2,1)S(1)} %convolution_convert_fusion.4), channel_id=1, source_target_pairs={{0,8},{2,10},{4,12},{6,14},{8,0},{10,2},{12,4},{14,6},{16,24},{18,... | collective-permute-start | bytes 1572872 | tf_op jit(solution)/shard_map/ppermute | solution.py:263
  113.9 12.8 %copy-start = (bf16[2048,1024]{1,0:T(8,128)(2,1)S(1)}, bf16[2048,1024]{1,0:T(8,128)(2,1)}, u32[]{:S(2)}) copy-start(bf16[2048,1024]{1,0:T(8,128)(2,1)} %param.11) | copy-start | bytes 12582916
  117.8 9.0 %collective-permute-start = (bf16[128,2048]{1,0:T(8,128)(2,1)S(1)}, bf16[128,2048]{1,0:T(8,128)(2,1)S(1)}, u32[]{:S(2)}, u32[]{:S(2)}) collective-permute-start(bf16[128,2048]{1,0:T(8,128)(2,1)S(1)} %convolution_convert_fusion), channel_id=1, source_target_pairs={{0,1},{1,0},{2,3},{3,2},{4,5},{5,4},{6,7},{7,6},{8,9},{9,8},{10,11... | collective-permute-start | bytes 1572872 | tf_op jit(solution)/shard_map/ppermute | solution.py:263
  117.8 20.6 %collective-permute-start.5 = (bf16[1024,384]{1,0:T(8,128)(2,1)S(1)}, bf16[1024,384]{1,0:T(8,128)(2,1)S(1)}, u32[]{:S(2)}, u32[]{:S(2)}) collective-permute-start(bf16[1024,384]{1,0:T(8,128)(2,1)S(1)} %copy-done.7), channel_id=1, source_target_pairs={{0,4},{2,6},{4,0},{6,2},{8,12},{10,14},{12,8},{14,10},{16,20},{18,... | collective-permute-start | bytes 2359304 | tf_op jit(solution)/shard_map/ppermute | solution.py:263
  118.8 21.0 %collective-permute-start.1 = (bf16[1024,384]{1,0:T(8,128)(2,1)S(1)}, bf16[1024,384]{1,0:T(8,128)(2,1)S(1)}, u32[]{:S(2)}, u32[]{:S(2)}) collective-permute-start(bf16[1024,384]{1,0:T(8,128)(2,1)S(1)} %copy-done.6), channel_id=1, source_target_pairs={{0,2},{2,0},{4,6},{6,4},{8,10},{10,8},{12,14},{14,12},{16,18},{18,... | collective-permute-start | bytes 2359304 | tf_op jit(solution)/shard_map/ppermute | solution.py:263
  124.4 14.1 %copy-start.4 = (bf16[256,2,2,1,2,128]{0,5,4,3,2,1:T(8,128)(2,1)S(1)}, bf16[256,2,2,1,2,128]{0,5,4,3,2,1:T(8,128)(2,1)}, u32[]{:S(2)}) copy-start(bf16[256,2,2,1,2,128]{0,5,4,3,2,1:T(8,128)(2,1)} %get-tuple-element.72) | copy-start | bytes 1572868
  124.4 12.7 %collective-permute-start.10 = (bf16[1,512,256]{2,1,0:T(8,128)(2,1)S(1)}, bf16[1,512,256]{2,1,0:T(8,128)(2,1)S(1)}, u32[]{:S(2)}, u32[]{:S(2)}) collective-permute-start(bf16[1,512,256]{2,1,0:T(8,128)(2,1)S(1)} %fusion.6), channel_id=1, source_target_pairs={{0,16},{2,18},{4,20},{6,22},{8,24},{10,26},{12,28},{14,30},{16,0},... | collective-permute-start | bytes 786440 | tf_op jit(solution)/shard_map/ppermute | solution.py:263
  137.1 2.7 %copy-start.3 = (bf16[256,2,2,2,1,128]{0,5,4,3,2,1:T(8,128)(2,1)S(1)}, bf16[256,2,2,2,1,128]{0,5,4,3,2,1:T(8,128)(2,1)}, u32[]{:S(2)}) copy-start(bf16[256,2,2,2,1,128]{0,5,4,3,2,1:T(8,128)(2,1)} %get-tuple-element.70) | copy-start | bytes 1572868
  137.2 6.0 %collective-permute-start.11 = (bf16[2,128,256]{2,1,0:T(8,128)(2,1)S(1)}, bf16[2,128,256]{2,1,0:T(8,128)(2,1)S(1)}, u32[]{:S(2)}, u32[]{:S(2)}) collective-permute-start(bf16[2,128,256]{2,1,0:T(8,128)(2,1)S(1)} %fusion.23), channel_id=1, source_target_pairs={{0,2},{2,0},{4,6},{6,4},{8,10},{10,8},{12,14},{14,12},{16,18},{18,... | collective-permute-start | bytes 393224 | tf_op jit(solution)/shard_map/ppermute | solution.py:263
  139.0 11.6 %collective-permute-start.6 = (bf16[4,128,384]{2,1,0:T(8,128)(2,1)S(1)}, bf16[4,128,384]{2,1,0:T(8,128)(2,1)S(1)}, u32[]{:S(2)}, u32[]{:S(2)}) collective-permute-start(bf16[4,128,384]{2,1,0:T(8,128)(2,1)S(1)} %fusion.1), channel_id=1, source_target_pairs={{0,2},{2,0},{4,6},{6,4},{8,10},{10,8},{12,14},{14,12},{16,18},{18,... | collective-permute-start | bytes 1179656 | tf_op jit(solution)/shard_map/ppermute | solution.py:263
  143.2 5.0 %collective-permute-start.12 = (bf16[1,128,256]{2,1,0:T(8,128)(2,1)S(1)}, bf16[1,128,256]{2,1,0:T(8,128)(2,1)S(1)}, u32[]{:S(2)}, u32[]{:S(2)}) collective-permute-start(bf16[1,128,256]{2,1,0:T(8,128)(2,1)S(1)} %dynamic-slice_convert_fusion.4), channel_id=1, source_target_pairs={{0,4},{2,6},{4,0},{6,2},{8,12},{10,14},{12,8},{14,10},{16,20},{18,... | collective-permute-start | bytes 196616 | tf_op jit(solution)/shard_map/ppermute | solution.py:263
  145.0 8.1 %collective-permute-start.2 = (bf16[4,128,384]{2,1,0:T(8,128)(2,1)S(1)}, bf16[4,128,384]{2,1,0:T(8,128)(2,1)S(1)}, u32[]{:S(2)}, u32[]{:S(2)}) collective-permute-start(bf16[4,128,384]{2,1,0:T(8,128)(2,1)S(1)} %fusion.2), channel_id=1, source_target_pairs={{0,4},{2,6},{4,0},{6,2},{8,12},{10,14},{12,8},{14,10},{16,20},{18,... | collective-permute-start | bytes 1179656 | tf_op jit(solution)/shard_map/ppermute | solution.py:263
  150.8 7.8 %collective-permute-start.7 = (bf16[2,128,384]{2,1,0:T(8,128)(2,1)S(1)}, bf16[2,128,384]{2,1,0:T(8,128)(2,1)S(1)}, u32[]{:S(2)}, u32[]{:S(2)}) collective-permute-start(bf16[2,128,384]{2,1,0:T(8,128)(2,1)S(1)} %fusion.12), channel_id=1, source_target_pairs={{0,8},{2,10},{4,12},{6,14},{8,0},{10,2},{12,4},{14,6},{16,24},{18,... | collective-permute-start | bytes 589832 | tf_op jit(solution)/shard_map/ppermute | solution.py:263
  153.3 8.8 %collective-permute-start.3 = (bf16[2,128,384]{2,1,0:T(8,128)(2,1)S(1)}, bf16[2,128,384]{2,1,0:T(8,128)(2,1)S(1)}, u32[]{:S(2)}, u32[]{:S(2)}) collective-permute-start(bf16[2,128,384]{2,1,0:T(8,128)(2,1)S(1)} %fusion.11), channel_id=1, source_target_pairs={{0,8},{2,10},{4,12},{6,14},{8,0},{10,2},{12,4},{14,6},{16,24},{18,... | collective-permute-start | bytes 589832 | tf_op jit(solution)/shard_map/ppermute | solution.py:263
  158.7 7.9 %collective-permute-start.8 = (bf16[1,128,384]{2,1,0:T(8,128)(2,1)S(1)}, bf16[1,128,384]{2,1,0:T(8,128)(2,1)S(1)}, u32[]{:S(2)}, u32[]{:S(2)}) collective-permute-start(bf16[1,128,384]{2,1,0:T(8,128)(2,1)S(1)} %dynamic-slice_convert_fusion.2), channel_id=1, source_target_pairs={{0,16},{2,18},{4,20},{6,22},{8,24},{10,26},{12,28},{14,30},{16,0},... | collective-permute-start | bytes 294920 | tf_op jit(solution)/shard_map/ppermute | solution.py:263
  162.1 6.6 %collective-permute-start.4 = (bf16[1,128,384]{2,1,0:T(8,128)(2,1)S(1)}, bf16[1,128,384]{2,1,0:T(8,128)(2,1)S(1)}, u32[]{:S(2)}, u32[]{:S(2)}) collective-permute-start(bf16[1,128,384]{2,1,0:T(8,128)(2,1)S(1)} %dynamic-slice_convert_fusion.3), channel_id=1, source_target_pairs={{0,16},{2,18},{4,20},{6,22},{8,24},{10,26},{12,28},{14,30},{16,0},... | collective-permute-start | bytes 294920 | tf_op jit(solution)/shard_map/ppermute | solution.py:263
